TPU v7x, 768 devices: a whole 4x8x12 slice. The times are simulated.
768 devices in a mesh: fs: 24 (over z, core), tp: 32 (over y, x).
Axes of the slice: x: 4, y: 8, z: 12, core: 2. Of those that a mesh axis runs over, the one named last changes fastest.
Arguments:
- block_in: bfloat16 [24576, 2304], P('fs'), may hold values from -6 to 6
- out_cot: bfloat16 [24576, 2304], P('fs'), may hold values from -6 to 6
- gated_out: bfloat16 [24576, 4608], P('fs', 'tp'), may hold values from -6 to 6
- gate_cot: bfloat16 [24576, 4608], P('fs', 'tp'), may hold values from -6 to 6
- factor_out: bfloat16 [2304, 192], P('fs'), may hold values from -0.104166667 to 0.104166667
- factor_z: bfloat16 [2304, 192], P('fs'), may hold values from -0.104166667 to 0.104166667
- weight_out: float32 [4608, 2304], P('tp', 'fs'), may hold values from -0.09375 to 0.09375
- weight_z: float32 [2304, 4608], P('fs', 'tp'), may hold values from -0.125 to 0.125
- first_out: float32 [4608, 192], P('tp', 'fs'), may hold values from -1254.13875 to 1254.13875
- second_out: float32 [4608, 192], P('tp', 'fs'), may hold values from 4915.2 to 122880
- first_z: float32 [192, 4608], P('fs', 'tp'), may hold values from -1254.13875 to 1254.13875
- second_z: float32 [192, 4608], P('fs', 'tp'), may hold values from 4915.2 to 122880
Outputs:
- step_out: float32 [4608, 2304], P('tp', 'fs')
- step_z: float32 [2304, 4608], P('fs', 'tp')
- new_first_out: float32 [4608, 192], P('tp', 'fs')
- new_second_out: float32 [4608, 192], P('tp', 'fs')
- new_first_z: float32 [192, 4608], P('fs', 'tp')
- new_second_z: float32 [192, 4608], P('fs', 'tp')
- copy_out: bfloat16 [4608, 2304], P('tp')
- copy_z: bfloat16 [2304, 4608], P(None, 'tp')
All inputs are finite; a program needn't handle non-finite values.
Results may differ from a plain program's by a relative error of at most 0.0018.
Values may be sent and summed in bfloat16 or wider, within the bound.
No kernel may reach another device: no remote copies, remote signals or barrier semaphores. Data moves between devices by JAX's collectives and lax.ppermute only.
A program may use at most 32 MiB of HBM per device.

v0:
```python
import jax
import jax.numpy as jnp
from jax import lax
from jax.sharding import Mesh
from jax.sharding import PartitionSpec as P

D = 2304
INNER = 4608
FS = ("fs_0", "fs_1")
FS_TP = ("fs_0", "fs_1", "tp_0", "tp_1")
TP = ("tp_0", "tp_1")


beta_first = 0.8
beta_second = 0.9
adam_eps = 1e-08
norm_eps = 1e-06
rate = 0.005


def in_order(tiles, dim):
    lengths = list(tiles.shape[1:])
    lengths[dim] *= tiles.shape[0]
    return jnp.moveaxis(tiles, 0, dim).reshape(lengths)


def gather_in_order(shard, axes, turns):
    tiles = shard[None]
    for k in turns:
        tiles = lax.all_gather(tiles, axes[k], axis=0, tiled=True)
    block = [lax.axis_size(axes[k]) for k in reversed(turns)]
    tiles = tiles.reshape(*block, *shard.shape)
    turned = sorted(range(len(turns)), key=lambda place: turns[len(turns) - 1 - place])
    return tiles.transpose(*turned, *range(len(turns), tiles.ndim)).reshape(-1, *shard.shape)


def gathered_by_axis(shard, axes, turns, dim):
    return in_order(gather_in_order(shard, axes, turns), dim)


def cut_along(shard, dim, count):
    lengths = shard.shape
    tiles = shard.reshape(*lengths[:dim], count, lengths[dim] // count, *lengths[dim + 1 :])
    return jnp.moveaxis(tiles, dim, 0)


def sent_and_summed(shard, axis, dim):
    tiles = cut_along(shard, dim, lax.axis_size(axis))
    arrived = lax.all_to_all(tiles, axis, split_axis=0, concat_axis=0, tiled=True)
    return arrived.sum(axis=0)


def rows_first(arrays, axis, dims):
    turned = [jnp.moveaxis(a, dim, 0) for a, dim in zip(arrays, dims)]
    both = jnp.concatenate([t.reshape(len(t), -1) for t in turned], axis=1)
    out, at, finished = (lax.all_gather(both, axis, axis=0, tiled=True), 0, [])
    for t, dim in zip(turned, dims):
        section = out[:, at : at + t[0].size].reshape(-1, *t.shape[1:])
        finished.append(jnp.moveaxis(section, 0, dim))
        at += t[0].size
    return tuple(finished)


def over_axes(shard, axes):
    for axis in axes:
        shard = lax.psum(shard, axis)
    return shard


def moments(first, second, gradient):
    new_first = beta_first * first + (1.0 - beta_first) * gradient
    new_second = beta_second * second + (1.0 - beta_second) * gradient * gradient
    return (new_first, new_second, new_first / (jnp.sqrt(new_second) + adam_eps))


def split_parts(values):
    high_part = values.astype(jnp.bfloat16)
    low_part = (values - high_part.astype(jnp.float32)).astype(jnp.bfloat16)
    return (high_part, low_part)


def per_device(
    block_in,
    out_cot,
    gated_out,
    gate_cot,
    factor_out,
    factor_z,
    weight_out,
    weight_z,
    first_out,
    second_out,
    first_z,
    second_z,
):
    sum_cot = jnp.dot(
        out_cot, gathered_by_axis(factor_out, FS, (0, 1), 0), preferred_element_type=jnp.float32
    )
    sum_input = jnp.dot(
        block_in, gathered_by_axis(factor_z, FS, (0, 1), 0), preferred_element_type=jnp.float32
    )
    cot_high, cot_low = split_parts(sum_cot)
    input_high, input_low = split_parts(sum_input)
    term_out = jnp.dot(gated_out.T, cot_high, preferred_element_type=jnp.float32) + jnp.dot(
        gated_out.T, cot_low, preferred_element_type=jnp.float32
    )
    term_z = jnp.dot(input_high.T, gate_cot, preferred_element_type=jnp.float32) + jnp.dot(
        input_low.T, gate_cot, preferred_element_type=jnp.float32
    )
    grad_out, grad_z = (sent_and_summed(term_out, FS, 1), sent_and_summed(term_z, FS, 0))
    new_first_out, new_second_out, part_out = moments(first_out, second_out, grad_out)
    new_first_z, new_second_z, part_z = moments(first_z, second_z, grad_z)
    dir_out, dir_z = rows_first((part_out, part_z), FS, (1, 0))
    update_out = jnp.dot(dir_out, factor_out.astype(jnp.float32).T, precision=lax.Precision.HIGHEST)
    update_z = jnp.dot(factor_z.astype(jnp.float32), dir_z, precision=lax.Precision.HIGHEST)
    total_out, total_z = (
        over_axes(jnp.sum(update_out * update_out), FS_TP),
        over_axes(jnp.sum(update_z * update_z), FS_TP),
    )
    entries = D * INNER
    step_out = update_out * lax.rsqrt(total_out / entries + norm_eps)
    step_z = update_z * lax.rsqrt(total_z / entries + norm_eps)
    fresh_out = (weight_out - rate * step_out).astype(jnp.bfloat16)
    fresh_z = (weight_z - rate * step_z).astype(jnp.bfloat16)
    copy_out, copy_z = rows_first((fresh_out, fresh_z), FS, (1, 0))
    return (
        step_out,
        step_z,
        new_first_out,
        new_second_out,
        new_first_z,
        new_second_z,
        copy_out,
        copy_z,
    )


def solution(mesh):
    finer = Mesh(mesh.devices.reshape(12, 2, 8, 4), ("fs_0", "fs_1", "tp_0", "tp_1"))
    placed = (
        P(FS, None),
        P(FS, None),
        P(FS, TP),
        P(FS, TP),
        P(FS, None),
        P(FS, None),
        P(TP, FS),
        P(FS, TP),
        P(TP, FS),
        P(TP, FS),
        P(FS, TP),
        P(FS, TP),
    )
    return jax.shard_map(
        per_device,
        mesh=finer,
        in_specs=placed,
        out_specs=(
            P(TP, FS),
            P(FS, TP),
            P(TP, FS),
            P(TP, FS),
            P(FS, TP),
            P(FS, TP),
            P(TP, None),
            P(None, TP),
        ),
        check_vma=False,
    )
```

profile of v0, /device:TPU:1, one launch (start us, length us, event | category | flops | bytes accessed | tf_op | source)
XLA Modules:
  0.0 266.0 jit_solution(9965768266253090050)
XLA Ops:
  7.2 0.0 copy-start
  7.2 31.6 %all-gather = bf16[1152,192]{1,0:T(8,128)(2,1)S(1)} all-gather(bf16[96,192]{1,0:T(8,128)(2,1)} %param.16), channel_id=2, replica_groups=mesh['fs_0'=12,'fs_1'=2,'tp_0'=8,'tp_1'=4] {'fs_0'}, dimensions={0}, use_global_device_ids=true | all-gather | bytes 479232 | tf_op jit(solution)/shard_map/all_gather | solution.py:30
  38.8 8.2 %all_gather.19 = bf16[24,96,192]{2,1,0:T(8,128)(2,1)S(1)} all-gather(bf16[12,96,192]{2,1,0:T(8,128)(2,1)S(1)} %bitcast.39), channel_id=1, replica_groups=mesh['fs_0'=12,'fs_1'=2,'tp_0'=8,'tp_1'=4] {'fs_1'}, dimensions={0}, use_global_device_ids=true | all-gather | bytes 1327104 | tf_op jit(solution)/shard_map/all_gather | solution.py:30
  47.0 1.1 copy.26
  48.1 0.9 reshape_reshape.6
  49.0 4.0 %fusion.17 = f32[1024,192]{0,1:T(8,128)S(1)} fusion(bf16[1024,2304]{1,0:T(8,128)(2,1)} %param.13, bf16[2304,192]{0,1:T(8,128)(2,1)S(1)} %reshape_reshape.6), kind=kOutput, calls=%fused_computation.34 | convolution fusion | flops 905969664 | bytes 6389760 | tf_op jit(solution)/shard_map/dot_general | solution.py:96
  53.0 0.0 copy-done
  53.0 0.0 copy-start.2
  53.0 0.3 fusion.9
  53.3 0.3 fusion
  53.6 0.8 copy.27
  54.4 3.9 %all-to-all-start = ((f32[24,144,8]{1,2,0:T(8,128)}), f32[24,144,8]{1,2,0:T(8,128)S(1)}, u32[]{:S(2)}, u32[]{:S(2)}) async-start(f32[24,144,8]{1,2,0:T(8,128)} %bitcast.5), calls=%async_computation | async-start | bytes 393216 | tf_op jit(solution)/shard_map/all_to_all | solution.py:49
  58.4 0.0 copy-done.2
  58.4 25.2 %all-gather.1 = bf16[1152,192]{1,0:T(8,128)(2,1)S(1)} all-gather(bf16[96,192]{1,0:T(8,128)(2,1)S(1)} %copy-done.2), channel_id=3, replica_groups=mesh['fs_0'=12,'fs_1'=2,'tp_0'=8,'tp_1'=4] {'fs_0'}, dimensions={0}, use_global_device_ids=true | all-gather | bytes 479232 | tf_op jit(solution)/shard_map/all_gather | solution.py:30
  83.6 7.6 %all_gather.21 = bf16[24,96,192]{2,1,0:T(8,128)(2,1)S(1)} all-gather(bf16[12,96,192]{2,1,0:T(8,128)(2,1)S(1)} %bitcast.40), channel_id=1, replica_groups=mesh['fs_0'=12,'fs_1'=2,'tp_0'=8,'tp_1'=4] {'fs_1'}, dimensions={0}, use_global_device_ids=true | all-gather | bytes 1327104 | tf_op jit(solution)/shard_map/all_gather | solution.py:30
  91.2 1.1 copy.28
  92.3 0.9 reshape_reshape.7
  93.2 0.0 copy-start.1
  93.2 4.0 %fusion.18 = f32[1024,192]{0,1:T(8,128)S(1)} fusion(bf16[1024,2304]{1,0:T(8,128)(2,1)} %param.12, bf16[2304,192]{0,1:T(8,128)(2,1)S(1)} %reshape_reshape.7), kind=kOutput, calls=%fused_computation.35 | convolution fusion | flops 905969664 | bytes 6389760 | tf_op jit(solution)/shard_map/dot_general | solution.py:99
  97.3 0.0 copy-done.1
  97.3 0.0 copy-start.6
  97.3 0.0 copy-start.7
  97.3 0.0 copy-start.8
  97.3 0.0 copy-start.9
  97.3 0.3 fusion.6
  97.6 0.0 copy-start.3
  97.6 0.0 copy-start.4
  97.6 0.0 copy-start.5
  97.6 0.3 convolution_add_fusion
  97.9 0.8 copy.29
  98.7 0.0 all-to-all-done
  98.7 6.9 %all-to-all-start.1 = ((f32[24,8,144]{2,1,0:T(8,128)}), f32[24,8,144]{2,1,0:T(8,128)S(1)}, u32[]{:S(2)}, u32[]{:S(2)}) async-start(f32[24,8,144]{2,1,0:T(8,128)} %bitcast.10), calls=%async_computation.1 | async-start | bytes 393216 | tf_op jit(solution)/shard_map/all_to_all | solution.py:49
  105.6 0.0 all-gather.4.cloned.1.call-start
  105.7 0.0 copy-done.6
  105.7 0.0 copy-done.7
  105.7 0.6 divide_bitcast_fusion
  106.3 13.0 %all-to-all-done.1 = f32[24,8,144]{2,1,0:T(8,128)S(1)} async-done(((f32[24,8,144]{2,1,0:T(8,128)}), f32[24,8,144]{2,1,0:T(8,128)S(1)}, u32[]{:S(2)}, u32[]{:S(2)}) %all-to-all-start.1) | async-done | bytes 110624 | tf_op jit(solution)/shard_map/all_to_all | solution.py:49
  119.3 0.0 copy-done.8
  119.3 0.0 copy-done.9
  119.3 0.6 add_divide_fusion
  120.0 0.1 pad_maximum_fusion.1
  120.0 23.7 %all_gather.22 = f32[192,288]{1,0:T(8,128)S(1)} all-gather(f32[8,288]{1,0:T(8,128)S(1)} %pad_maximum_fusion.1), channel_id=1, replica_groups=mesh['fs_0'=12,'fs_1'=2,'tp_0'=8,'tp_1'=4] {'fs_0','fs_1'}, dimensions={0}, use_global_device_ids=true | all-gather | bytes 230400 | tf_op jit(solution)/shard_map/all_gather | solution.py:56
  143.7 1.0 multiply_reduce_fusion
  144.7 0.0 copy-done.3
  144.7 0.9 multiply_reduce_fusion.1
  145.7 16.1 %all-reduce = (f32[]{:T(128)}, f32[]{:T(128)}) all-reduce(f32[]{:T(128)} %get-tuple-element.36, f32[]{:T(128)} %get-tuple-element.38), channel_id=1, replica_groups=mesh['fs_0'=12,'fs_1'=2,'tp_0'=8,'tp_1'=4] {'fs_0'}, use_global_device_ids=true, to_apply=%region_3.0 | all-reduce | flops 2 | bytes 16 | tf_op jit(solution)/shard_map/psum | solution.py:66
  161.8 8.4 %all-reduce.3 = (f32[]{:T(128)}, f32[]{:T(128)}) all-reduce(f32[]{:T(128)} %get-tuple-element.16, f32[]{:T(128)} %get-tuple-element.17), channel_id=1, replica_groups=mesh['fs_0'=12,'fs_1'=2,'tp_0'=8,'tp_1'=4] {'fs_1'}, use_global_device_ids=true, to_apply=%region_4.0 | all-reduce | flops 2 | bytes 16 | tf_op jit(solution)/shard_map/psum | solution.py:66
  170.2 14.7 %all-reduce.1 = (f32[]{:T(128)}, f32[]{:T(128)}) all-reduce(f32[]{:T(128)} %get-tuple-element.22, f32[]{:T(128)} %get-tuple-element.23), channel_id=1, replica_groups=mesh['fs_0'=12,'fs_1'=2,'tp_0'=8,'tp_1'=4] {'tp_0'}, use_global_device_ids=true, to_apply=%region_5.0 | all-reduce | flops 2 | bytes 16 | tf_op jit(solution)/shard_map/psum | solution.py:66
  184.9 9.1 %all-reduce.2 = (f32[]{:T(128)}, f32[]{:T(128)}) all-reduce(f32[]{:T(128)} %get-tuple-element.18, f32[]{:T(128)} %get-tuple-element.19), channel_id=1, replica_groups=mesh['fs_0'=12,'fs_1'=2,'tp_0'=8,'tp_1'=4] {'tp_1'}, use_global_device_ids=true, to_apply=%region_6.0 | all-reduce | flops 2 | bytes 16 | tf_op jit(solution)/shard_map/psum | solution.py:66
  195.4 0.0 copy-done.4
  195.4 0.6 fusion.11
  196.0 0.0 copy-done.5
  196.0 0.6 subtract_convert_fusion.4
  196.7 0.7 copy.30
  197.4 0.0 all-gather.4.cloned.1.call-update
  197.5 57.1 %all-gather.4.cloned.1.call-done = bf16[2304,288]{1,0:T(8,128)(2,1)} async-done(((bf16[96,288]{1,0:T(8,128)(2,1)}), bf16[2304,288]{1,0:T(8,128)(2,1)}) %all-gather.4.cloned.1.call-update) | async-done | bytes 1327120 | tf_op jit(solution)/shard_map/all_gather | solution.py:56
  254.5 2.2 fusion.16
  256.7 1.3 copy.32
  257.9 1.2 copy.31
  (3 shorter events, 0.1 us)
Async XLA Ops:
  7.2 45.9 %copy-start = (bf16[1024,144]{0,1:T(8,128)(2,1)S(1)}, bf16[1024,144]{0,1:T(8,128)(2,1)}, u32[]{:S(2)}) copy-start(bf16[1024,144]{0,1:T(8,128)(2,1)} %param.14) | copy-start | bytes 884740
  53.0 5.3 %copy-start.2 = (bf16[96,192]{1,0:T(8,128)(2,1)S(1)}, bf16[96,192]{1,0:T(8,128)(2,1)}, u32[]{:S(2)}) copy-start(bf16[96,192]{1,0:T(8,128)(2,1)} %param.17) | copy-start | bytes 110596
  54.4 44.3 %all-to-all-start = ((f32[24,144,8]{1,2,0:T(8,128)}), f32[24,144,8]{1,2,0:T(8,128)S(1)}, u32[]{:S(2)}, u32[]{:S(2)}) async-start(f32[24,144,8]{1,2,0:T(8,128)} %bitcast.5), calls=%async_computation | async-start | bytes 393216 | tf_op jit(solution)/shard_map/all_to_all | solution.py:49
  93.2 4.1 %copy-start.1 = (bf16[1024,144]{0,1:T(8,128)(2,1)S(1)}, bf16[1024,144]{0,1:T(8,128)(2,1)}, u32[]{:S(2)}) copy-start(bf16[1024,144]{0,1:T(8,128)(2,1)} %param.15) | copy-start | bytes 884740
  97.3 8.4 %copy-start.6 = (f32[144,8]{0,1:T(8,128)S(1)}, f32[144,8]{0,1:T(8,128)}, u32[]{:S(2)}) copy-start(f32[144,8]{0,1:T(8,128)} %param.21) | copy-start | bytes 13828
  97.3 8.4 %copy-start.7 = (f32[144,8]{0,1:T(8,128)S(1)}, f32[144,8]{0,1:T(8,128)}, u32[]{:S(2)}) copy-start(f32[144,8]{0,1:T(8,128)} %param.20) | copy-start | bytes 13828
  97.3 22.0 %copy-start.8 = (f32[8,144]{1,0:T(8,128)S(1)}, f32[8,144]{1,0:T(8,128)}, u32[]{:S(2)}) copy-start(f32[8,144]{1,0:T(8,128)} %param.23) | copy-start | bytes 13828
  97.3 22.0 %copy-start.9 = (f32[8,144]{1,0:T(8,128)S(1)}, f32[8,144]{1,0:T(8,128)}, u32[]{:S(2)}) copy-start(f32[8,144]{1,0:T(8,128)} %param.22) | copy-start | bytes 13828
  97.6 47.1 %copy-start.3 = (bf16[96,192]{1,0:T(8,128)(2,1)S(1)}, bf16[96,192]{1,0:T(8,128)(2,1)}, u32[]{:S(2)}) copy-start(bf16[96,192]{1,0:T(8,128)(2,1)} %param.16) | copy-start | bytes 110596
  97.6 97.7 %copy-start.4 = (f32[144,96]{1,0:T(8,128)S(1)}, f32[144,96]{1,0:T(8,128)}, u32[]{:S(2)}) copy-start(f32[144,96]{1,0:T(8,128)} %param.18) | copy-start | bytes 165892
  97.6 98.4 %copy-start.5 = (f32[96,144]{0,1:T(8,128)S(1)}, f32[96,144]{0,1:T(8,128)}, u32[]{:S(2)}) copy-start(f32[96,144]{0,1:T(8,128)} %param.19) | copy-start | bytes 165892
  98.7 20.6 %all-to-all-start.1 = ((f32[24,8,144]{2,1,0:T(8,128)}), f32[24,8,144]{2,1,0:T(8,128)S(1)}, u32[]{:S(2)}, u32[]{:S(2)}) async-start(f32[24,8,144]{2,1,0:T(8,128)} %bitcast.10), calls=%async_computation.1 | async-start | bytes 393216 | tf_op jit(solution)/shard_map/all_to_all | solution.py:49
  105.6 148.9 %all-gather.4.cloned.1.call-start = ((), (), s32[]{:S(2)}) async-start(), calls=%async_computation.2 | async-start | bytes 1843200 | tf_op jit(solution)/shard_map/all_gather | solution.py:56
Sparse Core Ops, SparseCore 0:
  197.6 56.8 all-gather.3
where the time goes:
time: 266 us
  blocking collectives  145 us (55%)
  waiting for transfers between devices  70.1 us (26%)
  between operations  15.6 us (6%)
  matrix products  11.2 us (4%)
  local copies, waits for them, and re-layouts  11.1 us (4%)
  starting transfers between devices  10.8 us (4%)
  other arithmetic  2.66 us (1%)
    all_gather x4, blocking collectives, gather_in_order(): tiles = lax.all_gather(tiles, axes[k], axis=0, tiled=True)  72.6 us
    all_gather x1, waiting for transfers between devices, rows_first(): out, at, finished = (lax.all_gather(both, axis, axis=0, tiled=True), 0, [])  57.1 us
    psum x4, blocking collectives, over_axes(): shard = lax.psum(shard, axis)  48.3 us
    all_gather x1, blocking collectives, rows_first(): out, at, finished = (lax.all_gather(both, axis, axis=0, tiled=True), 0, [])  23.7 us
    all_to_all x2, waiting for transfers between devices, sent_and_summed(): lax.all_to_all(tiles, axis, split_axis=0, concat_axis=0, tiled=True)  13 us
    all_to_all x2, starting transfers between devices, sent_and_summed(): lax.all_to_all(tiles, axis, split_axis=0, concat_axis=0, tiled=True)  10.8 us
  transfers between devices with their start and end apart: 3, of which 2 were waited for; matrix products, arithmetic and copies ran while one was open for 3% of the time, Pallas kernels for 0%

commit v1 on v0

v1 whole, which is shorter than its diff:
```python
import jax
import jax.numpy as jnp
from jax import lax
from jax.experimental import pallas as pl
from jax.experimental.pallas import tpu as pltpu
from jax.sharding import Mesh
from jax.sharding import PartitionSpec as P

D = 2304
INNER = 4608
RANK = 192
FS = ("z", "core")
TP = ("y", "x")
RINGS, CORES = 12, 2
PARTS = RINGS * CORES
TPS = 32
CHUNKS = 4
FLYING = 2

beta_first = 0.8
beta_second = 0.9
adam_eps = 1e-08
norm_eps = 1e-06
rate = 0.005

VMEM = pl.BlockSpec(memory_space=pltpu.VMEM)
SMEM = pl.BlockSpec(memory_space=pltpu.SMEM)
HBM = pl.BlockSpec(memory_space=pltpu.HBM)
FLAT = (((1,), (0,)), ((), ()))
TURNED = (((1,), (1,)), ((), ()))


def dot(a, b, dims):
    return lax.dot_general(a, b, dims, preferred_element_type=jnp.float32)


def in_hbm(value):
    return pltpu.with_memory_space_constraint(value, pltpu.HBM)


def in_vmem(value):
    return pltpu.with_memory_space_constraint(value, pltpu.VMEM)


def split_parts(values):
    high_part = values.astype(jnp.bfloat16)
    return high_part, (values - high_part.astype(jnp.float32)).astype(jnp.bfloat16)


def call(kernel, outs, specs, mib, scratch=()):
    return pl.pallas_call(
        kernel,
        out_shape=[
            out[2](out[0], out[1]) if len(out) == 3 else jax.ShapeDtypeStruct(*out) for out in outs
        ],
        in_specs=specs,
        out_specs=[HBM if pltpu.HBM in out else VMEM for out in outs],
        scratch_shapes=scratch,
        compiler_params=pltpu.CompilerParams(vmem_limit_bytes=mib * 1024 * 1024),
    )


def gradient_kernel(
    core, cot, inp, own, other, gated, gate, partial, factor_out, factor_z, kept_out, kept_z,
    tokens, gates, highs, lows, sems, gate_sems, kept_sems,
):
    sides = ((cot, gated, factor_out), (inp, gate, factor_z))
    moves = []
    for k, (source, _, _) in enumerate(sides):
        for c in range(CHUNKS):
            height = tokens.shape[1] // CHUNKS
            at = pl.ds(height * c, height)
            moves.append((k, at, pltpu.make_async_copy(source.at[at], tokens.at[k, at], sems.at[k, c])))
    gate_moves = [
        pltpu.make_async_copy(turned, gates.at[k], gate_sems.at[k]) for k, (_, turned, _) in enumerate(sides)
    ]
    for _, _, move in moves[:FLYING]:
        move.start()

    rows = own.shape[0] // RINGS
    here = core[0] * rows
    there = rows - here
    for z in range(RINGS):
        for shard, place in ((own, here), (other, there)):
            block = shard[rows * z : rows * (z + 1), :]
            at = pl.ds(pl.multiple_of(2 * rows * z + place, 32), rows)
            factor_out[at, :] = block[:, :RANK]
            factor_z[at, :] = block[:, RANK:]

    keeps = [
        pltpu.make_async_copy(factor, kept, kept_sems.at[k])
        for k, (factor, kept) in enumerate(((factor_out, kept_out), (factor_z, kept_z)))
    ]
    width = gated.shape[0]
    for n, (k, at, move) in enumerate(moves):
        move.wait()
        if n + FLYING < len(moves):
            moves[n + FLYING][2].start()
        elif n + FLYING < len(moves) + 2:
            gate_moves[n + FLYING - len(moves)].start()
            keeps[n + FLYING - len(moves)].start()
        high, low = split_parts(dot(tokens[k, at, :], sides[k][2][...], FLAT))
        highs[k, at, :] = high
        lows[k, at, :] = low
    for k, move in enumerate(gate_moves):
        move.wait()
        total = dot(gates[k], highs[k], FLAT) + dot(gates[k], lows[k], FLAT)
        partial[:, k * width : (k + 1) * width] = total.T
    for keep in keeps:
        keep.wait()


def moments_kernel(arrived, first_out, second_out, first_z, second_z, *outs):
    total = jnp.sum(arrived[...], axis=0)
    width = first_out.shape[1]
    ratios = outs[-1]
    for k, (first, second) in enumerate(((first_out, second_out), (first_z, second_z))):
        gradient = total[:, k * width : (k + 1) * width]
        new_first = beta_first * first[...] + (1.0 - beta_first) * gradient
        new_second = beta_second * second[...] + (1.0 - beta_second) * gradient * gradient
        outs[2 * k][...] = new_first
        outs[2 * k + 1][...] = new_second
        ratio = new_first / (jnp.sqrt(new_second) + adam_eps)
        ratios[..., k * width : (k + 1) * width] = jnp.broadcast_to(ratio, ratios.shape[:-1] + (width,))


def turned_parts(ratios, width):
    turned = ratios[...].T
    return [split_parts(turned[k * width : (k + 1) * width]) for k in range(2)]


def sums_kernel(ratios, factor_out, factor_z, sums):
    totals = []
    for (high, low), factor in zip(turned_parts(ratios, ratios.shape[1] // 2), (factor_out, factor_z)):
        update = dot(high, factor[...], TURNED) + dot(low, factor[...], TURNED)
        totals.append(jnp.sum(jnp.sum(update * update, axis=0, keepdims=True), axis=1, keepdims=True))
    lane = lax.broadcasted_iota(jnp.int32, (1, 128), 1)
    row = jnp.where(lane < 64, totals[0], totals[1])
    sums[...] = jnp.broadcast_to(row[None], sums.shape)


def update_kernel(
    place, ratios, kept_out, kept_z, weights, wide, narrow, full, factors, blocks, factor_sems, sem
):
    width, columns = narrow.shape[0] // 2, narrow.shape[1]
    moves = [
        pltpu.make_async_copy(kept, factors.at[k], factor_sems.at[k])
        for k, kept in enumerate((kept_out, kept_z))
    ]
    move = pltpu.make_async_copy(weights, blocks, sem)
    for each in (*moves, move):
        each.start()
    for k, (high, low) in enumerate(turned_parts(ratios, width)):
        rows = pl.ds(k * width, width)
        moves[k].wait()
        wide[rows, :] = dot(high, factors[k], TURNED) + dot(low, factors[k], TURNED)
        mine = factors[k, pl.ds(pl.multiple_of(place[0] * columns, 32), columns), :]
        narrow[rows, :] = dot(high, mine, TURNED) + dot(low, mine, TURNED)
    move.wait()
    for k in range(PARTS):
        full[:, k * columns : (k + 1) * columns] = blocks[k]


def final_kernel(sums, wide, narrow, full, copy_out, copy_z, step_out, step_z):
    width = step_out.shape[0]
    total = jnp.sum(sums[...], axis=0)
    scales = lax.rsqrt(total / (D * INNER) + norm_eps)
    for k, (copy, step) in enumerate(((copy_out, step_out), (copy_z, step_z))):
        scale = scales[:, 64 * k : 64 * k + 1]
        rows = pl.ds(k * width, width)
        step[...] = narrow[rows, :] * scale
        copy[...] = (full[rows, :] - rate * (wide[rows, :] * scale)).astype(jnp.bfloat16)


def per_device(
    block_in, out_cot, gated_out, gate_cot, factor_out, factor_z,
    weight_out, weight_z, first_out, second_out, first_z, second_z,
):
    f32, bf16 = jnp.float32, jnp.bfloat16
    width, columns = weight_out.shape
    ranks = first_z.shape[0]
    tokens = block_in.shape[0]
    core = lax.axis_index("core").reshape(1).astype(jnp.int32)
    place = lax.axis_index(FS).reshape(1).astype(jnp.int32)

    own = lax.all_gather(jnp.concatenate([factor_out, factor_z], axis=1), "z", axis=0, tiled=True)
    if SC_LATE:
        own, weight_out, weight_z = lax.optimization_barrier((own, weight_out, weight_z))
    other = lax.ppermute(own, "core", [(0, 1), (1, 0)])
    weights = jnp.concatenate([weight_out, weight_z.T], axis=0)
    weights = lax.all_gather(weights, FS, axis=0, tiled=True).reshape(PARTS, 2 * width, columns)

    partial, full_out, full_z, kept_out, kept_z = call(
        gradient_kernel,
        [((RANK, 2 * width), f32)] + [((D, RANK), bf16, pltpu.VMEM)] * 2 + [((D, RANK), bf16, pltpu.HBM)] * 2,
        [SMEM, HBM, HBM, VMEM, VMEM, HBM, HBM],
        24,
        [
            pltpu.VMEM((2, tokens, D), bf16),
            pltpu.VMEM((2, width, tokens), bf16),
            pltpu.VMEM((2, tokens, RANK), bf16),
            pltpu.VMEM((2, tokens, RANK), bf16),
            pltpu.SemaphoreType.DMA((2, CHUNKS)),
            pltpu.SemaphoreType.DMA((2,)),
            pltpu.SemaphoreType.DMA((2,)),
        ],
    )(core, in_hbm(out_cot), in_hbm(block_in), in_vmem(own), in_vmem(other), in_hbm(gated_out.T), in_hbm(gate_cot.T))
    arrived = lax.all_to_all(
        partial.reshape(PARTS, ranks, 2 * width), FS, split_axis=0, concat_axis=0, tiled=True
    )
    small = ((ranks, width), f32)
    lead = (PARTS,) if DIR_A2A else ()
    *news, ratios = call(moments_kernel, [small] * 4 + [(lead + (ranks, 2 * width), f32)], [VMEM] * 5, 4)(
        arrived, first_out.T, second_out.T, first_z, second_z
    )
    if DIR_A2A:
        ratios = lax.all_to_all(ratios, FS, split_axis=0, concat_axis=0, tiled=True).reshape(RANK, 2 * width)
    else:
        ratios = lax.all_gather(ratios, FS, axis=0, tiled=True)
    (sums,) = call(sums_kernel, [((TPS, 1, 128), f32)], [VMEM] * 3, 8)(
        ratios, in_vmem(full_out), in_vmem(full_z)
    )
    sums = lax.all_to_all(sums, TP, split_axis=0, concat_axis=0, tiled=True)
    wide, narrow, full = call(
        update_kernel,
        [((2 * width, D), f32, pltpu.VMEM), ((2 * width, columns), f32, pltpu.VMEM), ((2 * width, D), f32, pltpu.VMEM)],
        [SMEM, VMEM, HBM, HBM, HBM],
        16,
        [
            pltpu.VMEM((2, D, RANK), bf16),
            pltpu.VMEM((PARTS, 2 * width, columns), f32),
            pltpu.SemaphoreType.DMA((2,)),
            pltpu.SemaphoreType.DMA,
        ],
    )(place, ratios, in_hbm(kept_out), in_hbm(kept_z), in_hbm(weights))
    copy_out, copy_z, step_out, step_z = call(
        final_kernel,
        [((width, D), bf16), ((width, D), bf16), ((width, columns), f32), ((width, columns), f32)],
        [VMEM] * 4,
        4,
    )(sums, in_vmem(wide), in_vmem(narrow), in_vmem(full))
    return (
        step_out, step_z.T, news[0].T, news[1].T, news[2], news[3], copy_out, copy_z.T,
    )


SC_LATE = True
DIR_A2A = True


def solution(mesh):
    finer = Mesh(mesh.devices.reshape(RINGS, CORES, 8, 4), FS + TP)
    rows, both, turned = P(FS, None), P(FS, TP), P(TP, FS)
    return jax.shard_map(
        per_device,
        mesh=finer,
        in_specs=(
            rows, rows, both, both, rows, rows, turned, both, turned, turned, both, both,
        ),
        out_specs=(turned, both, turned, turned, both, both, P(TP, None), P(None, TP)),
        check_vma=False,
    )
```

time: 266 us -> 140 us (0.53)
  blocking collectives: 145 us -> 78.2 us
  waiting for transfers between devices: 70.1 us -> 3.99 us
  Pallas kernels: 0 us -> 18.9 us
  matrix products: 11.2 us -> 0 us
  local copies, waits for them, and re-layouts: 11.1 us -> 3.26 us
  starting transfers between devices: 10.8 us -> 17.4 us
    all_gather x5 -> x1, blocking collectives: 96.3 us -> 33.3 us  [per_device(): lax.all_gather(jnp.concatenate([factor_out, factor_z], axis=1), 'z', axis...]
    all_gather x1, waiting for transfers between devices: 57.1 us -> 0.02 us  [per_device(): lax.all_gather(weights, FS, axis=0, tiled=True)]
    psum x4 -> x0, blocking collectives: 48.3 us -> none  [over_axes(): shard = lax.psum(shard, axis)]
    all_to_all x0 -> x2, blocking collectives: none -> 44.9 us  [the longest x1 22.7 us: per_device(): lax.all_to_all(ratios, FS, split_axis=0, concat_axis=0, tiled=True)]
    pallas_call x0 -> x5, Pallas kernels: none -> 18.9 us  [the longest x1 9.17 us: per_device(): call(gradient_kernel, [((RANK, 2 * width), f32)] + [((D, RANK), bf16, plt...]
    dot_general x8 -> x0, matrix products: 11.2 us -> none  [the longest x1 4.05 us: per_device(): jnp.dot(block_in, gathered_by_axis(factor_z, FS, (0, 1), 0), preferred_el...]
    all_to_all x2 -> x1, waiting for transfers between devices: 13 us -> 1.93 us  [per_device(): sums = lax.all_to_all(sums, TP, split_axis=0, concat_axis=0, tiled=True)]
    ppermute x0 -> x1, starting transfers between devices: none -> 8.07 us  [per_device(): other = lax.ppermute(own, 'core', [(0, 1), (1, 0)])]
  transfers between devices with their start and end apart: 3 -> 3, of which waited for: 2 -> 2; matrix products, arithmetic and copies ran while one was open for 3% -> 0% of each run, Pallas kernels for 0% -> 13%
where the time goes in v1:
time: 140 us; the launch traced here: 138 us
  blocking collectives  78.2 us (56%)
  Pallas kernels  18.9 us (13%)
  starting transfers between devices  17.4 us (12%)
  between operations  14.1 us (10%)
  waiting for transfers between devices  3.99 us (3%)
  local copies, waits for them, and re-layouts  3.26 us (2%)
  other arithmetic  2.5 us (2%)
    all_gather x1, blocking collectives, per_device(): lax.all_gather(jnp.concatenate([factor_out, factor_z], axis=1), 'z', axis...  33.3 us
    all_to_all x1, blocking collectives, per_device(): lax.all_to_all(ratios, FS, split_axis=0, concat_axis=0, tiled=True)  22.7 us
    all_to_all x1, blocking collectives, per_device(): lax.all_to_all(partial.reshape(PARTS, ranks, 2 * width), FS, split_axis=0...  22.2 us
    all_to_all x1, starting transfers between devices, per_device(): sums = lax.all_to_all(sums, TP, split_axis=0, concat_axis=0, tiled=True)  9.28 us
    pallas_call x1, Pallas kernels, per_device(): call(gradient_kernel, [((RANK, 2 * width), f32)] + [((D, RANK), bf16, plt...  9.17 us
    ppermute x1, starting transfers between devices, per_device(): other = lax.ppermute(own, 'core', [(0, 1), (1, 0)])  8.07 us
    pallas_call x1, Pallas kernels, per_device(): call(update_kernel, [((2 * width, D), f32, pltpu.VMEM), ((2 * width, colu...  5.05 us
    unnamed x12, local copies, waits for them, and re-layouts  3.26 us
  transfers between devices with their start and end apart: 3, of which 2 were waited for; matrix products, arithmetic and copies ran while one was open for 0% of the time, Pallas kernels for 13%

profile of v1, /device:TPU:1, one launch (start us, length us, event | category | flops | bytes accessed | tf_op | source)
XLA Modules:
  0.0 138.4 jit_solution(2758549020564962365)
XLA Ops:
  7.2 0.0 all-gather.2.cloned.1.call-start
  7.2 0.9 pad_maximum_fusion.1
  8.1 33.3 %all_gather.6.own = bf16[1152,384]{1,0:T(8,128)(2,1)S(1)} all-gather(bf16[96,384]{1,0:T(8,128)(2,1)S(1)} %pad_maximum_fusion.1), channel_id=1, replica_groups=mesh['z'=12,'core'=2,'y'=8,'x'=4] {'z'}, dimensions={0}, use_global_device_ids=true | all-gather | bytes 958464 | tf_op jit(solution)/shard_map/all_gather | solution.py:186
  41.4 1.6 %pad_maximum_fusion = f32[288,96]{1,0:T(8,128)} fusion(f32[144,96]{1,0:T(8,128)} %bitcast.22, f32[144,96]{1,0:T(8,128)} %param.18), kind=kLoop, calls=%fused_computation | loop fusion | flops 27648 | bytes 221184 | tf_op jit(solution)/shard_map/concatenate | solution.py:190
  43.0 0.0 all-gather.2.cloned.1.call-update
  43.1 8.1 %collective-permute-start = (bf16[1152,384]{1,0:T(8,128)(2,1)S(1)}, bf16[1152,384]{1,0:T(8,128)(2,1)S(1)}, u32[]{:S(2)}, u32[]{:S(2)}) collective-permute-start(bf16[1152,384]{1,0:T(8,128)(2,1)S(1)} %all_gather.6.own), channel_id=1, source_target_pairs={{0,32},{32,0},{1,33},{33,1},{2,34},{34,2},{3,35},{35,3},{4,36},{36... | collective-permute-start | bytes 2654216 | tf_op jit(solution)/shard_map/ppermute | solution.py:189
  51.1 2.0 %collective-permute-done.other = bf16[1152,384]{1,0:T(8,128)(2,1)S(1)} collective-permute-done((bf16[1152,384]{1,0:T(8,128)(2,1)S(1)}, bf16[1152,384]{1,0:T(8,128)(2,1)S(1)}, u32[]{:S(2)}, u32[]{:S(2)}) %collective-permute-start) | collective-permute-done | bytes 884768 | tf_op jit(solution)/shard_map/ppermute | solution.py:189
  53.2 0.0 copy-start.2
  53.2 0.0 copy-start.3
  53.2 0.0 copy-start.4
  53.2 0.0 copy-start.5
  53.2 9.2 %shard_map.179 = (f32[192,288]{1,0:T(8,128)S(1)}, bf16[2304,192]{1,0:T(8,128)(2,1)S(1)}, bf16[2304,192]{1,0:T(8,128)(2,1)S(1)}, bf16[2304,192]{1,0:T(8,128)(2,1)}, bf16[2304,192]{1,0:T(8,128)(2,1)}) custom-call(s32[1]{0:T(128)} %bitcast.core, bf16[1024,2304]{1,0:T(8,128)(2,1)} %cot.1, bf16[1024,2304]{1,0:T(8,128)(2,1)} %inp.1, ...), custom_call_target="tpu_custom_call" | custom-call | tf_op jit(solution)/shard_map/pallas_call | solution.py:193
  62.4 22.2 %all_to_all.15.arrived = f32[24,8,288]{2,1,0:T(8,128)S(1)} all-to-all(f32[24,8,288]{2,1,0:T(8,128)S(1)} %bitcast.16), channel_id=1, replica_groups=mesh['z'=12,'core'=2,'y'=8,'x'=4] {'z','core'}, dimensions={0} | all-to-all | bytes 442368 | tf_op jit(solution)/shard_map/all_to_all | solution.py:208
  84.6 0.0 copy-done.2
  84.6 0.0 copy-done.3
  84.6 0.0 copy-done.4
  84.6 0.0 copy-done.5
  84.6 0.7 shard_map.180
  85.3 22.7 %all_to_all.16 = f32[24,8,288]{2,1,0:T(8,128)S(1)} all-to-all(f32[24,8,288]{2,1,0:T(8,128)S(1)} %get-tuple-element.30), channel_id=1, replica_groups=mesh['z'=12,'core'=2,'y'=8,'x'=4] {'z','core'}, dimensions={0} | all-to-all | bytes 442368 | tf_op jit(solution)/shard_map/all_to_all | solution.py:217
  108.0 2.4 %shard_map.181 = f32[32,1,128]{2,1,0:T(1,128)} custom-call(f32[192,288]{1,0:T(8,128)S(1)} %bitcast.14, bf16[2304,192]{1,0:T(8,128)(2,1)S(1)} %get-tuple-element.31.factor_out, bf16[2304,192]{1,0:T(8,128)(2,1)S(1)} %get-tuple-element.32.factor_z), custom_call_target="tpu_custom_call" | custom-call | tf_op jit(solution)/shard_map/pallas_call | solution.py:220
  110.4 9.3 %all-to-all-start.2 = ((f32[32,1,128]{2,1,0:T(1,128)}), f32[32,1,128]{2,1,0:T(1,128)S(1)}, u32[]{:S(2)}, u32[]{:S(2)}) async-start(f32[32,1,128]{2,1,0:T(1,128)} %shard_map.181), calls=%async_computation.2 | async-start | bytes 32768 | tf_op jit(solution)/shard_map/all_to_all | solution.py:223
  119.7 0.0 all-gather.2.cloned.1.call-done
  119.7 5.1 %shard_map.182 = (f32[288,2304]{1,0:T(8,128)S(1)}, f32[288,96]{1,0:T(8,128)S(1)}, f32[288,2304]{1,0:T(8,128)S(1)}) custom-call(s32[1]{0:T(128)} %bitcast.7.place, f32[192,288]{1,0:T(8,128)S(1)} %bitcast.15, bf16[2304,192]{1,0:T(8,128)(2,1)} %get-tuple-element.33.kept_out, bf16[2304,192]{1,0:T(8,128)(2,1)} %get-tuple-element.34.kept_z, f32[24,288,96]{2,1,0:T(8,128)} %bitcast.19), custom_call_target="tpu_custom_call" | custom-call | tf_op jit(solution)/shard_map/pallas_call | solution.py:224
  124.8 0.0 copy-start
  124.8 1.5 %copy-done = f32[288,2304]{1,0:T(8,128)} copy-done((f32[288,2304]{1,0:T(8,128)}, f32[288,2304]{1,0:T(8,128)S(1)}, u32[]{:S(2)}) %copy-start) | copy-done | bytes 2654232
  126.3 1.9 %all-to-all-done.2.sums = f32[32,1,128]{2,1,0:T(1,128)S(1)} async-done(((f32[32,1,128]{2,1,0:T(1,128)}), f32[32,1,128]{2,1,0:T(1,128)S(1)}, u32[]{:S(2)}, u32[]{:S(2)}) %all-to-all-start.2) | async-done | bytes 16416 | tf_op jit(solution)/shard_map/all_to_all | solution.py:223
  128.2 0.0 copy-start.1
  128.2 1.7 %copy-done.1 = f32[288,2304]{1,0:T(8,128)S(1)} copy-done((f32[288,2304]{1,0:T(8,128)S(1)}, f32[288,2304]{1,0:T(8,128)}, u32[]{:S(2)}) %copy-start.1) | copy-done | bytes 2654232
  130.0 1.6 %shard_map.183 = (bf16[144,2304]{1,0:T(8,128)(2,1)}, bf16[144,2304]{1,0:T(8,128)(2,1)}, f32[144,96]{1,0:T(8,128)}, f32[144,96]{1,0:T(8,128)}) custom-call(f32[32,1,128]{2,1,0:T(1,128)S(1)} %all-to-all-done.2.sums, f32[288,2304]{1,0:T(8,128)S(1)} %get-tuple-element.37.wide, f32[288,96]{1,0:T(8,128)S(1)} %get-tuple-element.38.narrow, f32[288,2304]{1,0:T(8,128)S(1)} %copy-done.1), custom_call_target="tpu_custom_call" | custom-call | tf_op jit(solution)/shard_map/pallas_call | solution.py:236
Async XLA Ops:
  7.2 112.6 %all-gather.2.cloned.1.call-start = ((), (), s32[]{:S(2)}) async-start(), calls=%async_computation.3 | async-start | bytes 3686400 | tf_op jit(solution)/shard_map/all_gather | solution.py:191
  43.1 10.1 %collective-permute-start = (bf16[1152,384]{1,0:T(8,128)(2,1)S(1)}, bf16[1152,384]{1,0:T(8,128)(2,1)S(1)}, u32[]{:S(2)}, u32[]{:S(2)}) collective-permute-start(bf16[1152,384]{1,0:T(8,128)(2,1)S(1)} %all_gather.6.own), channel_id=1, source_target_pairs={{0,32},{32,0},{1,33},{33,1},{2,34},{34,2},{3,35},{35,3},{4,36},{36... | collective-permute-start | bytes 2654216 | tf_op jit(solution)/shard_map/ppermute | solution.py:189
  53.2 31.4 %copy-start.2 = (f32[144,8]{0,1:T(8,128)S(1)}, f32[144,8]{0,1:T(8,128)}, u32[]{:S(2)}) copy-start(f32[144,8]{0,1:T(8,128)} %param.20) | copy-start | bytes 13828
  53.2 31.4 %copy-start.3 = (f32[144,8]{0,1:T(8,128)S(1)}, f32[144,8]{0,1:T(8,128)}, u32[]{:S(2)}) copy-start(f32[144,8]{0,1:T(8,128)} %param.21) | copy-start | bytes 13828
  53.2 31.4 %copy-start.4 = (f32[8,144]{1,0:T(8,128)S(1)}, f32[8,144]{1,0:T(8,128)}, u32[]{:S(2)}) copy-start(f32[8,144]{1,0:T(8,128)} %first_z.1) | copy-start | bytes 13828
  53.2 31.4 %copy-start.5 = (f32[8,144]{1,0:T(8,128)S(1)}, f32[8,144]{1,0:T(8,128)}, u32[]{:S(2)}) copy-start(f32[8,144]{1,0:T(8,128)} %second_z.1) | copy-start | bytes 13828
  110.4 17.8 %all-to-all-start.2 = ((f32[32,1,128]{2,1,0:T(1,128)}), f32[32,1,128]{2,1,0:T(1,128)S(1)}, u32[]{:S(2)}, u32[]{:S(2)}) async-start(f32[32,1,128]{2,1,0:T(1,128)} %shard_map.181), calls=%async_computation.2 | async-start | bytes 32768 | tf_op jit(solution)/shard_map/all_to_all | solution.py:223
  124.8 1.5 %copy-start = (f32[288,2304]{1,0:T(8,128)}, f32[288,2304]{1,0:T(8,128)S(1)}, u32[]{:S(2)}) copy-start(f32[288,2304]{1,0:T(8,128)S(1)} %get-tuple-element.39.full) | copy-start | bytes 7962628
  128.2 1.8 %copy-start.1 = (f32[288,2304]{1,0:T(8,128)S(1)}, f32[288,2304]{1,0:T(8,128)}, u32[]{:S(2)}) copy-start(f32[288,2304]{1,0:T(8,128)} %copy-done) | copy-start | bytes 7962628
Sparse Core Ops, SparseCore 0:
  43.2 73.4 all-gather.1

commit v2 on v1

v2 whole, which is shorter than its diff:
```python
import jax
import jax.numpy as jnp
from jax import lax
from jax.experimental import pallas as pl
from jax.experimental.pallas import tpu as pltpu
from jax.sharding import Mesh
from jax.sharding import PartitionSpec as P

D = 2304
INNER = 4608
RANK = 192
FS = ("z", "core")
TP = ("y", "x")
RINGS, CORES = 12, 2
PARTS = RINGS * CORES
TPS = 32
CHUNKS = 4
LANES = 128

beta_first = 0.8
beta_second = 0.9
adam_eps = 1e-08
norm_eps = 1e-06
rate = 0.005

VMEM = pl.BlockSpec(memory_space=pltpu.VMEM)
SMEM = pl.BlockSpec(memory_space=pltpu.SMEM)
HBM = pl.BlockSpec(memory_space=pltpu.HBM)
FLAT = (((1,), (0,)), ((), ()))
TURNED = (((1,), (1,)), ((), ()))


def dot(a, b, dims):
    return lax.dot_general(a, b, dims, preferred_element_type=jnp.float32)


def in_hbm(value):
    return pltpu.with_memory_space_constraint(value, pltpu.HBM)


def in_vmem(value):
    return pltpu.with_memory_space_constraint(value, pltpu.VMEM)


def split_parts(values):
    high_part = values.astype(jnp.bfloat16)
    return high_part, (values - high_part.astype(jnp.float32)).astype(jnp.bfloat16)


def call(kernel, outs, specs, mib, scratch=()):
    return pl.pallas_call(
        kernel,
        out_shape=[
            out[2](out[0], out[1]) if len(out) == 3 else jax.ShapeDtypeStruct(*out) for out in outs
        ],
        in_specs=specs,
        out_specs=[HBM if pltpu.HBM in out else VMEM for out in outs],
        scratch_shapes=scratch,
        compiler_params=pltpu.CompilerParams(vmem_limit_bytes=mib * 1024 * 1024),
    )


def to_tiles(values, k, tiles, rest):
    ranks, spare = RANK // PARTS, values.shape[1] - LANES
    each = tiles.shape[0] // PARTS
    for p in range(PARTS):
        tiles[each * p + ranks * k : each * p + ranks * (k + 1), :] = values[ranks * p : ranks * (p + 1), :LANES]
    rest[:, :spare] = values[:, LANES:]
    row = [rest[pl.ds(r, PARTS, stride=ranks), :][:, :spare] for r in range(ranks)]
    tiles[pl.ds(2 * ranks + k, PARTS, stride=each), :] = jnp.concatenate(row, axis=1)


def from_tiles(tiles, k, values, rest):
    ranks, spare = RANK // PARTS, values.shape[1] - LANES
    each = tiles.shape[0] // PARTS
    for p in range(PARTS):
        values[ranks * p : ranks * (p + 1), :LANES] = tiles[each * p + ranks * k : each * p + ranks * (k + 1), :]
    row = tiles[pl.ds(2 * ranks + k, PARTS, stride=each), :]
    for r in range(ranks):
        rest[pl.ds(r, PARTS, stride=ranks), :] = jnp.concatenate([row[:, spare * r :], row[:, : spare * r]], axis=1) if r else row
    values[:, LANES:] = rest[:, :spare]


def pack_kernel(factor_out, factor_z, weight_out, weight_z, packed, weights, parts, both, sems):
    height = weight_out.shape[0]
    moves = [
        pltpu.make_async_copy(weight_out, both.at[pl.ds(0, height)], sems.at[2]),
        pltpu.make_async_copy(weight_z, both.at[pl.ds(height, height)], sems.at[3]),
        pltpu.make_async_copy(factor_out, parts.at[0], sems.at[0]),
        pltpu.make_async_copy(factor_z, parts.at[1], sems.at[1]),
    ]
    for move in moves:
        move.start()
    for move in moves[:2]:
        move.wait()
    out = pltpu.make_async_copy(both, weights, sems.at[2])
    out.start()
    for k in range(2):
        moves[2 + k].wait()
        packed[:, k * RANK : (k + 1) * RANK] = parts[k]
    out.wait()


def stage_kernel(source, kept, sems):
    height = source.shape[0] // CHUNKS
    moves = [
        pltpu.make_async_copy(
            source.at[pl.ds(height * c, height)], kept.at[pl.ds(height * c, height)], sems.at[c]
        )
        for c in range(CHUNKS)
    ]
    for move in moves:
        move.start()
    for move in moves:
        move.wait()


def gradient_kernel(
    cot, inp, own, other, gated, gate, partial, factor_out, factor_z, tokens, gates, projected, rest, sems, gate_sems
):
    moves = []
    for c in range(CHUNKS):
        height = tokens.shape[0] // CHUNKS
        at = pl.ds(height * c, height)
        moves.append(pltpu.make_async_copy(inp.at[at], tokens.at[at], sems.at[c]))
    gate_moves = [
        pltpu.make_async_copy(turned, gates.at[k], gate_sems.at[k]) for k, turned in enumerate((gated, gate))
    ]
    for move in (gate_moves[0], *moves, gate_moves[1]):
        move.start()

    rows = own.shape[0] // RINGS
    here = lax.axis_index("core") * rows
    there = rows - here
    for z in range(RINGS):
        for shard, place in ((own, here), (other, there)):
            block = shard[rows * z : rows * (z + 1), :]
            at = pl.ds(pl.multiple_of(2 * rows * z + place, 32), rows)
            factor_out[at, :] = block[:, :RANK]
            factor_z[at, :] = block[:, RANK:]

    for k, (side, factor) in enumerate(((cot, factor_out), (tokens, factor_z))):
        if k == 1:
            for move in moves:
                move.wait()
        for c in range(CHUNKS):
            at = pl.ds(height * c, height)
            projected[at, :] = dot(side[at, :], factor[...], FLAT)
        high, low = split_parts(projected[...])
        gate_moves[k].wait()
        total = dot(gates[k], high, FLAT) + dot(gates[k], low, FLAT)
        to_tiles(total.T, k, partial, rest)


def moments_kernel(arrived, first_out, second_out, first_z, second_z, *refs):
    *outs, tiles, part, side = refs
    ranks, width = first_out.shape
    spare = width - LANES
    each = arrived.shape[0] // PARTS
    total = arrived[:each, :]
    for p in range(1, PARTS):
        total = total + arrived[each * p : each * (p + 1), :]
    part[...] = total
    for k, (first, second) in enumerate(((first_out, second_out), (first_z, second_z))):
        last = 2 * ranks + k
        side[:, :LANES] = part[ranks * k : ranks * (k + 1), :]
        for r in range(ranks):
            side[r : r + 1, LANES:] = part[last : last + 1, spare * r : spare * (r + 1)]
        gradient = side[...]
        new_first = beta_first * first[...] + (1.0 - beta_first) * gradient
        new_second = beta_second * second[...] + (1.0 - beta_second) * gradient * gradient
        outs[2 * k][...] = new_first
        outs[2 * k + 1][...] = new_second
        ratio = new_first / (jnp.sqrt(new_second) + adam_eps)
        part[ranks * k : ranks * (k + 1), :] = ratio[:, :LANES]
        for r in range(ranks):
            part[last : last + 1, spare * r : spare * (r + 1)] = ratio[r : r + 1, LANES:]
    for p in range(PARTS):
        tiles[each * p : each * (p + 1), :] = part[...]


def ordered_kernel(weights, ordered, blocks, full, sems):
    columns = blocks.shape[2]
    half = PARTS // 2
    moves = [
        pltpu.make_async_copy(
            weights.at[pl.ds(half * k, half)], blocks.at[pl.ds(half * k, half)], sems.at[k]
        )
        for k in range(2)
    ]
    for move in moves:
        move.start()
    for k in range(PARTS):
        if k % half == 0:
            moves[k // half].wait()
        full[:, k * columns : (k + 1) * columns] = blocks[k]
    out = pltpu.make_async_copy(full, ordered, sems.at[0])
    out.start()
    out.wait()


def update_kernel(tiles, factor_out, factor_z, ordered, wide, narrow, full, sums, ratios, rest, sem):
    width, columns = narrow.shape[0] // 2, narrow.shape[1]
    move = pltpu.make_async_copy(ordered, full, sem)
    move.start()
    totals = []
    for k, factor in enumerate((factor_out, factor_z)):
        rows = pl.ds(k * width, width)
        from_tiles(tiles, k, ratios, rest)
        high, low = split_parts(ratios[...].T)
        update = dot(high, factor[...], TURNED) + dot(low, factor[...], TURNED)
        wide[rows, :] = update
        totals.append(jnp.sum(jnp.sum(update * update, axis=0, keepdims=True), axis=1, keepdims=True))
        mine = factor[pl.ds(pl.multiple_of(lax.axis_index(FS) * columns, 32), columns), :]
        narrow[rows, :] = dot(high, mine, TURNED) + dot(low, mine, TURNED)
    lane = lax.broadcasted_iota(jnp.int32, (1, 128), 1)
    row = jnp.where(lane < 64, totals[0], totals[1])
    sums[...] = jnp.broadcast_to(row[None], sums.shape)
    move.wait()


def final_kernel(sums, wide, narrow, full, copy_out, copy_z, step_out, step_z):
    width = step_out.shape[0]
    total = jnp.sum(sums[...], axis=0)
    scales = lax.rsqrt(total / (D * INNER) + norm_eps)
    for k, (copy, step) in enumerate(((copy_out, step_out), (copy_z, step_z))):
        scale = scales[:, 64 * k : 64 * k + 1]
        rows = pl.ds(k * width, width)
        step[...] = narrow[rows, :] * scale
        copy[...] = (full[rows, :] - rate * (wide[rows, :] * scale)).astype(jnp.bfloat16)


def per_device(
    block_in, out_cot, gated_out, gate_cot, factor_out, factor_z,
    weight_out, weight_z, first_out, second_out, first_z, second_z,
):
    f32, bf16 = jnp.float32, jnp.bfloat16
    width, columns = weight_out.shape
    ranks = first_z.shape[0]
    tokens = block_in.shape[0]

    rows_in_all = 2 * RANK * width // LANES

    def exchanged(tiles):
        shape = (PARTS, rows_in_all // PARTS // 2, 2, LANES)
        moved = lax.all_to_all(tiles.reshape(shape), FS, split_axis=0, concat_axis=0, tiled=True)
        return moved.reshape(tiles.shape)

    packed, weights = call(
        pack_kernel,
        [((columns, 2 * RANK), bf16), ((2 * width, columns), f32, pltpu.HBM)],
        [HBM] * 4,
        4,
        [
            pltpu.VMEM((2, columns, RANK), bf16),
            pltpu.VMEM((2 * width, columns), f32),
            pltpu.SemaphoreType.DMA((4,)),
        ],
    )(in_hbm(factor_out), in_hbm(factor_z), in_hbm(weight_out), in_hbm(weight_z.T))
    weights = lax.all_gather(weights, FS, axis=0, tiled=True).reshape(PARTS, 2 * width, columns)
    own = lax.all_gather(packed, "z", axis=0, tiled=True)
    other = lax.ppermute(own, "core", [(0, 1), (1, 0)])
    _, source = lax.optimization_barrier((own, out_cot))
    (staged,) = call(
        stage_kernel,
        [((tokens, D), bf16, pltpu.VMEM)],
        [HBM],
        2,
        [pltpu.SemaphoreType.DMA((CHUNKS,))],
    )(in_hbm(source))

    partial, full_out, full_z = call(
        gradient_kernel,
        [((rows_in_all, LANES), f32)] + [((D, RANK), bf16, pltpu.VMEM)] * 2,
        [VMEM, HBM, VMEM, VMEM, HBM, HBM],
        24,
        [
            pltpu.VMEM((tokens, D), bf16),
            pltpu.VMEM((2, width, tokens), bf16),
            pltpu.VMEM((tokens, RANK), f32),
            pltpu.VMEM((RANK, LANES), f32),
            pltpu.SemaphoreType.DMA((CHUNKS,)),
            pltpu.SemaphoreType.DMA((2,)),
        ],
    )(in_vmem(staged), in_hbm(block_in), in_vmem(own), in_vmem(other), in_hbm(gated_out.T), in_hbm(gate_cot.T))
    arrived = exchanged(partial)
    small = ((ranks, width), f32)
    *news, ratios = call(
        moments_kernel,
        [small] * 4 + [((rows_in_all, LANES), f32)],
        [VMEM] * 5,
        4,
        [pltpu.VMEM((rows_in_all // PARTS, LANES), f32), pltpu.VMEM((ranks, width), f32)],
    )(arrived, first_out.T, second_out.T, first_z, second_z)
    ratios = exchanged(ratios)
    (ordered,) = call(
        ordered_kernel,
        [((2 * width, D), f32, pltpu.HBM)],
        [HBM],
        16,
        [
            pltpu.VMEM((PARTS, 2 * width, columns), f32),
            pltpu.VMEM((2 * width, D), f32),
            pltpu.SemaphoreType.DMA((2,)),
        ],
    )(in_hbm(weights))
    wide, narrow, full, sums = call(
        update_kernel,
        [
            ((2 * width, D), f32, pltpu.VMEM),
            ((2 * width, columns), f32, pltpu.VMEM),
            ((2 * width, D), f32, pltpu.VMEM),
            ((TPS, 1, 128), f32),
        ],
        [VMEM, VMEM, VMEM, HBM],
        8,
        [pltpu.VMEM((RANK, width), f32), pltpu.VMEM((RANK, LANES), f32), pltpu.SemaphoreType.DMA],
    )(ratios, in_vmem(full_out), in_vmem(full_z), in_hbm(ordered))
    sums = lax.all_to_all(sums, TP, split_axis=0, concat_axis=0, tiled=True)
    copy_out, copy_z, step_out, step_z = call(
        final_kernel,
        [((width, D), bf16), ((width, D), bf16), ((width, columns), f32), ((width, columns), f32)],
        [VMEM] * 4,
        4,
    )(sums, in_vmem(wide), in_vmem(narrow), in_vmem(full))
    return (
        step_out, step_z.T, news[0].T, news[1].T, news[2], news[3], copy_out, copy_z.T,
    )


def solution(mesh):
    finer = Mesh(mesh.devices.reshape(RINGS, CORES, 8, 4), FS + TP)
    rows, both, turned = P(FS, None), P(FS, TP), P(TP, FS)
    return jax.shard_map(
        per_device,
        mesh=finer,
        in_specs=(
            rows, rows, both, both, rows, rows, turned, both, turned, turned, both, both,
        ),
        out_specs=(turned, both, turned, turned, both, both, P(TP, None), P(None, TP)),
        check_vma=False,
    )
```

time: 140 us -> 129 us (0.921)
  blocking collectives: 78.2 us -> 70.7 us
  waiting for transfers between devices: 3.99 us -> 10.4 us
  local copies, waits for them, and re-layouts: 3.26 us -> 0.03 us
  starting transfers between devices: 17.4 us -> 14.2 us
  other arithmetic: 2.5 us -> 0 us
    all_to_all x2, blocking collectives: 44.9 us -> 36.1 us  [the longest x1 18.3 us: exchanged(): lax.all_to_all(tiles.reshape(shape), FS, split_axis=0, concat_axis=0, til...]
    all_to_all x1, waiting for transfers between devices: 1.93 us -> 10.4 us  [exchanged(): lax.all_to_all(tiles.reshape(shape), FS, split_axis=0, concat_axis=0, til...]
    all_to_all x1, starting transfers between devices: 9.28 us -> 5.99 us  [exchanged(): lax.all_to_all(tiles.reshape(shape), FS, split_axis=0, concat_axis=0, til...]
    unnamed x12 -> x8, local copies, waits for them, and re-layouts: 3.26 us -> 0.03 us
    pallas_call x1, Pallas kernels: 5.05 us -> 1.97 us  [per_device(): call(update_kernel, [((2 * width, D), f32, pltpu.VMEM), ((2 * width, colu...]
    pallas_call x3 -> x5, Pallas kernels: 12.3 us -> 14.9 us  [the longest x1 5.99 us: per_device(): call(gradient_kernel, [((rows_in_all, LANES), f32)] + [((D, RANK), bf16,...]
    concatenate x2 -> x0, other arithmetic: 2.5 us -> none  [the longest x1 1.59 us: per_device(): weights = jnp.concatenate([weight_out, weight_z.T], axis=0)]
    ppermute x1, waiting for transfers between devices: 2.02 us -> 0.01 us  [per_device(): other = lax.ppermute(own, 'core', [(0, 1), (1, 0)])]
  transfers between devices with their start and end apart: 3 -> 3, of which waited for: 2 -> 1; matrix products, arithmetic and copies ran while one was open for 0% -> 0% of each run, Pallas kernels for 13% -> 10%
where the time goes in v2:
time: 129 us; the launch traced here: 128 us
  blocking collectives  70.7 us (55%)
  Pallas kernels  18.5 us (14%)
  starting transfers between devices  14.2 us (11%)
  between operations  14.1 us (11%)
  waiting for transfers between devices  10.4 us (8%)
    all_gather x1, blocking collectives, per_device(): own = lax.all_gather(packed, 'z', axis=0, tiled=True)  34.6 us
    all_to_all x1, blocking collectives, exchanged(): lax.all_to_all(tiles.reshape(shape), FS, split_axis=0, concat_axis=0, til...  18.3 us
    all_to_all x1, blocking collectives, per_device(): sums = lax.all_to_all(sums, TP, split_axis=0, concat_axis=0, tiled=True)  17.8 us
    all_to_all x1, waiting for transfers between devices, exchanged(): lax.all_to_all(tiles.reshape(shape), FS, split_axis=0, concat_axis=0, til...  10.4 us
    ppermute x1, starting transfers between devices, per_device(): other = lax.ppermute(own, 'core', [(0, 1), (1, 0)])  8.17 us
    all_to_all x1, starting transfers between devices, exchanged(): lax.all_to_all(tiles.reshape(shape), FS, split_axis=0, concat_axis=0, til...  5.99 us
    pallas_call x1, Pallas kernels, per_device(): call(gradient_kernel, [((rows_in_all, LANES), f32)] + [((D, RANK), bf16,...  5.99 us
    pallas_call x1, Pallas kernels, per_device(): call(ordered_kernel, [((2 * width, D), f32, pltpu.HBM)], [HBM], 16, [pltp...  3.94 us
  transfers between devices with their start and end apart: 3, of which 1 were waited for; matrix products, arithmetic and copies ran while one was open for 0% of the time, Pallas kernels for 10%

profile of v2, /device:TPU:1, one launch (start us, length us, event | category | flops | bytes accessed | tf_op | source)
XLA Modules:
  0.0 128.0 jit_solution(11462343194642162722)
XLA Ops:
  7.2 0.0 all-gather.2.cloned.1.call-start
  7.2 1.6 %shard_map.179 = (bf16[96,384]{1,0:T(8,128)(2,1)S(1)}, f32[288,96]{1,0:T(8,128)}) custom-call(bf16[96,192]{1,0:T(8,128)(2,1)} %factor_out.1, bf16[96,192]{1,0:T(8,128)(2,1)} %factor_z.1, f32[144,96]{1,0:T(8,128)} %weight_out.1, f32[144,96]{1,0:T(8,128)} %bitcast.22), custom_call_target="tpu_custom_call" | custom-call | tf_op jit(solution)/shard_map/pallas_call | solution.py:249
  8.8 0.0 all-gather.2.cloned.1.call-update
  8.9 34.6 %all_gather.6.own = bf16[1152,384]{1,0:T(8,128)(2,1)S(1)} all-gather(bf16[96,384]{1,0:T(8,128)(2,1)S(1)} %get-tuple-element.27), channel_id=1, replica_groups=mesh['z'=12,'core'=2,'y'=8,'x'=4] {'z'}, dimensions={0}, use_global_device_ids=true | all-gather | bytes 958464 | tf_op jit(solution)/shard_map/all_gather | solution.py:261
  43.4 8.2 %collective-permute-start = (bf16[1152,384]{1,0:T(8,128)(2,1)S(1)}, bf16[1152,384]{1,0:T(8,128)(2,1)S(1)}, u32[]{:S(2)}, u32[]{:S(2)}) collective-permute-start(bf16[1152,384]{1,0:T(8,128)(2,1)S(1)} %all_gather.6.own), channel_id=1, source_target_pairs={{0,32},{32,0},{1,33},{33,1},{2,34},{34,2},{3,35},{35,3},{4,36},{36... | collective-permute-start | bytes 2654216 | tf_op jit(solution)/shard_map/ppermute | solution.py:262
  51.6 2.4 %shard_map.180.cot = bf16[1024,2304]{1,0:T(8,128)(2,1)S(1)} custom-call(bf16[1024,2304]{1,0:T(8,128)(2,1)} %source), custom_call_target="tpu_custom_call" | custom-call | tf_op jit(solution)/shard_map/pallas_call | solution.py:264
  54.0 0.0 collective-permute-done.other
  54.0 0.0 copy-start
  54.0 0.0 copy-start.1
  54.1 0.0 copy-start.2
  54.1 0.0 copy-start.3
  54.1 6.0 %shard_map.181 = (f32[432,128]{1,0:T(8,128)S(1)}, bf16[2304,192]{1,0:T(8,128)(2,1)S(1)}, bf16[2304,192]{1,0:T(8,128)(2,1)S(1)}) custom-call(bf16[1024,2304]{1,0:T(8,128)(2,1)S(1)} %shard_map.180.cot, bf16[1024,2304]{1,0:T(8,128)(2,1)} %inp.1, bf16[1152,384]{1,0:T(8,128)(2,1)S(1)} %all_gather.6.own, bf16[1152,384]{1,0:T(8,128)(2,1)S(1)} %collective-permute-done.other, ...), custom_call_target="tpu_custom_call" | custom-call | tf_op jit(solution)/shard_map/pallas_call | solution.py:272
  60.1 18.3 %all_to_all.15 = f32[24,9,2,128]{3,2,1,0:T(2,128)S(1)} all-to-all(f32[24,9,2,128]{3,2,1,0:T(2,128)S(1)} %bitcast.16), channel_id=1, replica_groups=mesh['z'=12,'core'=2,'y'=8,'x'=4] {'z','core'}, dimensions={0} | all-to-all | bytes 442368 | tf_op jit(solution)/shard_map/all_to_all | solution.py:246
  78.4 0.0 copy-done
  78.4 0.0 copy-done.1
  78.4 0.0 copy-done.2
  78.4 0.0 copy-done.3
  78.4 0.9 shard_map.182
  79.3 6.0 %all-to-all-start.1 = ((f32[24,9,2,128]{3,2,1,0:T(2,128)}), f32[24,9,2,128]{3,2,1,0:T(2,128)S(1)}, u32[]{:S(2)}, u32[]{:S(2)}) async-start(f32[24,9,2,128]{3,2,1,0:T(2,128)} %bitcast.7), calls=%async_computation.1 | async-start | bytes 442368 | tf_op jit(solution)/shard_map/all_to_all | solution.py:246
  85.3 0.0 all-gather.2.cloned.1.call-done
  85.4 3.9 %shard_map.183.ordered = f32[288,2304]{1,0:T(8,128)} custom-call(f32[24,288,96]{2,1,0:T(8,128)} %bitcast.19), custom_call_target="tpu_custom_call" | custom-call | tf_op jit(solution)/shard_map/pallas_call | solution.py:296
  89.3 10.4 %all-to-all-done.1 = f32[24,9,2,128]{3,2,1,0:T(2,128)S(1)} async-done(((f32[24,9,2,128]{3,2,1,0:T(2,128)}), f32[24,9,2,128]{3,2,1,0:T(2,128)S(1)}, u32[]{:S(2)}, u32[]{:S(2)}) %all-to-all-start.1) | async-done | bytes 221216 | tf_op jit(solution)/shard_map/all_to_all | solution.py:246
  99.7 2.0 %shard_map.184 = (f32[288,2304]{1,0:T(8,128)S(1)}, f32[288,96]{1,0:T(8,128)S(1)}, f32[288,2304]{1,0:T(8,128)S(1)}, f32[32,1,128]{2,1,0:T(1,128)S(1)}) custom-call(f32[432,128]{1,0:T(8,128)S(1)} %bitcast.15, bf16[2304,192]{1,0:T(8,128)(2,1)S(1)} %get-tuple-element.31.factor_out, bf16[2304,192]{1,0:T(8,128)(2,1)S(1)} %get-tuple-element.32.factor_z, ...), custom_call_target="tpu_custom_call" | custom-call | tf_op jit(solution)/shard_map/pallas_call | solution.py:307
  101.7 17.8 %all_to_all.16.sums = f32[32,1,128]{2,1,0:T(1,128)S(1)} all-to-all(f32[32,1,128]{2,1,0:T(1,128)S(1)} %get-tuple-element.34), channel_id=1, replica_groups=mesh['z'=12,'core'=2,'y'=8,'x'=4] {'y','x'}, dimensions={0} | all-to-all | bytes 32768 | tf_op jit(solution)/shard_map/all_to_all | solution.py:319
  119.5 1.7 %shard_map.185 = (bf16[144,2304]{1,0:T(8,128)(2,1)}, bf16[144,2304]{1,0:T(8,128)(2,1)}, f32[144,96]{1,0:T(8,128)}, f32[144,96]{1,0:T(8,128)}) custom-call(f32[32,1,128]{2,1,0:T(1,128)S(1)} %all_to_all.16.sums, f32[288,2304]{1,0:T(8,128)S(1)} %get-tuple-element.35.wide, f32[288,96]{1,0:T(8,128)S(1)} %get-tuple-element.36.narrow, ...), custom_call_target="tpu_custom_call" | custom-call | tf_op jit(solution)/shard_map/pallas_call | solution.py:320
Async XLA Ops:
  7.2 78.2 %all-gather.2.cloned.1.call-start = ((), (), s32[]{:S(2)}) async-start(), calls=%async_computation.3 | async-start | bytes 3686400 | tf_op jit(solution)/shard_map/all_gather | solution.py:260
  43.4 10.6 %collective-permute-start = (bf16[1152,384]{1,0:T(8,128)(2,1)S(1)}, bf16[1152,384]{1,0:T(8,128)(2,1)S(1)}, u32[]{:S(2)}, u32[]{:S(2)}) collective-permute-start(bf16[1152,384]{1,0:T(8,128)(2,1)S(1)} %all_gather.6.own), channel_id=1, source_target_pairs={{0,32},{32,0},{1,33},{33,1},{2,34},{34,2},{3,35},{35,3},{4,36},{36... | collective-permute-start | bytes 2654216 | tf_op jit(solution)/shard_map/ppermute | solution.py:262
  54.0 24.4 %copy-start = (f32[144,8]{0,1:T(8,128)S(1)}, f32[144,8]{0,1:T(8,128)}, u32[]{:S(2)}) copy-start(f32[144,8]{0,1:T(8,128)} %param.20) | copy-start | bytes 13828
  54.0 24.4 %copy-start.1 = (f32[144,8]{0,1:T(8,128)S(1)}, f32[144,8]{0,1:T(8,128)}, u32[]{:S(2)}) copy-start(f32[144,8]{0,1:T(8,128)} %param.21) | copy-start | bytes 13828
  54.1 24.4 %copy-start.2 = (f32[8,144]{1,0:T(8,128)S(1)}, f32[8,144]{1,0:T(8,128)}, u32[]{:S(2)}) copy-start(f32[8,144]{1,0:T(8,128)} %first_z.1) | copy-start | bytes 13828
  54.1 24.3 %copy-start.3 = (f32[8,144]{1,0:T(8,128)S(1)}, f32[8,144]{1,0:T(8,128)}, u32[]{:S(2)}) copy-start(f32[8,144]{1,0:T(8,128)} %second_z.1) | copy-start | bytes 13828
  79.3 20.4 %all-to-all-start.1 = ((f32[24,9,2,128]{3,2,1,0:T(2,128)}), f32[24,9,2,128]{3,2,1,0:T(2,128)S(1)}, u32[]{:S(2)}, u32[]{:S(2)}) async-start(f32[24,9,2,128]{3,2,1,0:T(2,128)} %bitcast.7), calls=%async_computation.1 | async-start | bytes 442368 | tf_op jit(solution)/shard_map/all_to_all | solution.py:246
Sparse Core Ops, SparseCore 0:
  11.0 72.6 all-gather.1

commit v3 on v2

--- a/solution.py
+++ b/solution.py
@@ -15,6 +15,7 @@
 PARTS = RINGS * CORES
 TPS = 32
 CHUNKS = 4
+BANDS = 3
 LANES = 128
 
 beta_first = 0.8
@@ -81,8 +82,8 @@
     values[:, LANES:] = rest[:, :spare]
 
 
-def pack_kernel(factor_out, factor_z, weight_out, weight_z, packed, weights, parts, both, sems):
-    height = weight_out.shape[0]
+def pack_kernel(factor_out, factor_z, weight_out, weight_z, packed, weights, parts, both, dense, sems):
+    height, columns = weight_out.shape
     moves = [
         pltpu.make_async_copy(weight_out, both.at[pl.ds(0, height)], sems.at[2]),
         pltpu.make_async_copy(weight_z, both.at[pl.ds(height, height)], sems.at[3]),
@@ -93,7 +94,12 @@
         move.start()
     for move in moves[:2]:
         move.wait()
-    out = pltpu.make_async_copy(both, weights, sems.at[2])
+    rows, spare = dense.shape[0], LANES - columns
+    dense[:, :columns] = both[:rows, :]
+    quarter = 2 * height - rows
+    for j in range(rows // quarter):
+        dense[quarter * j : quarter * (j + 1), columns:] = both[rows:, spare * j : spare * (j + 1)]
+    out = pltpu.make_async_copy(dense, weights, sems.at[2])
     out.start()
     for k in range(2):
         moves[2 + k].wait()
@@ -180,7 +186,8 @@
 
 
 def ordered_kernel(weights, ordered, blocks, full, sems):
-    columns = blocks.shape[2]
+    rows, columns = blocks.shape[1], full.shape[1] // PARTS
+    quarter, spare = full.shape[0] - rows, LANES - columns
     half = PARTS // 2
     moves = [
         pltpu.make_async_copy(
@@ -193,7 +200,12 @@
     for k in range(PARTS):
         if k % half == 0:
             moves[k // half].wait()
-        full[:, k * columns : (k + 1) * columns] = blocks[k]
+        at = k * columns
+        full[:rows, at : at + columns] = blocks[k, :, :columns]
+        for j in range(rows // quarter):
+            full[rows:, at + spare * j : at + spare * (j + 1)] = blocks[
+                k, quarter * j : quarter * (j + 1), columns:
+            ]
     out = pltpu.make_async_copy(full, ordered, sems.at[0])
     out.start()
     out.wait()
@@ -207,27 +219,46 @@
     for k, factor in enumerate((factor_out, factor_z)):
         rows = pl.ds(k * width, width)
         from_tiles(tiles, k, ratios, rest)
-        high, low = split_parts(ratios[...].T)
-        update = dot(high, factor[...], TURNED) + dot(low, factor[...], TURNED)
-        wide[rows, :] = update
-        totals.append(jnp.sum(jnp.sum(update * update, axis=0, keepdims=True), axis=1, keepdims=True))
+        both = jnp.concatenate(split_parts(ratios[...].T), axis=0)
+        squares = jnp.zeros((1, 2 * LANES), jnp.float32)
+        for n in range(0, D, 2 * LANES):
+            terms = dot(both, factor[n : n + 2 * LANES, :], TURNED)
+            update = terms[:width] + terms[width:]
+            wide[rows, n : n + 2 * LANES] = update
+            squares = squares + jnp.sum(update * update, axis=0, keepdims=True)
+        totals.append(jnp.sum(squares, axis=1, keepdims=True))
         mine = factor[pl.ds(pl.multiple_of(lax.axis_index(FS) * columns, 32), columns), :]
-        narrow[rows, :] = dot(high, mine, TURNED) + dot(low, mine, TURNED)
-    lane = lax.broadcasted_iota(jnp.int32, (1, 128), 1)
-    row = jnp.where(lane < 64, totals[0], totals[1])
+        terms = dot(both, mine, TURNED)
+        narrow[rows, :] = terms[:width] + terms[width:]
+    lane = lax.broadcasted_iota(jnp.int32, (1, LANES), 1)
+    row = jnp.where(lane < LANES // 2, totals[0], totals[1])
     sums[...] = jnp.broadcast_to(row[None], sums.shape)
     move.wait()
 
 
-def final_kernel(sums, wide, narrow, full, copy_out, copy_z, step_out, step_z):
+def final_kernel(
+    sums, wide, narrow, full, copy_out, copy_z, step_out, step_z, copies, steps, copy_sems, step_sems
+):
     width = step_out.shape[0]
+    height = width // BANDS
     total = jnp.sum(sums[...], axis=0)
     scales = lax.rsqrt(total / (D * INNER) + norm_eps)
+    moves = []
     for k, (copy, step) in enumerate(((copy_out, step_out), (copy_z, step_z))):
-        scale = scales[:, 64 * k : 64 * k + 1]
+        scale = scales[:, LANES // 2 * k : LANES // 2 * k + 1]
+        for c in range(BANDS):
+            rows = pl.ds(k * width + height * c, height)
+            copies[rows, :] = (full[rows, :] - rate * (wide[rows, :] * scale)).astype(jnp.bfloat16)
+            moves.append(
+                pltpu.make_async_copy(copies.at[rows], copy.at[pl.ds(height * c, height)], copy_sems.at[k, c])
+            )
+            moves[-1].start()
         rows = pl.ds(k * width, width)
-        step[...] = narrow[rows, :] * scale
-        copy[...] = (full[rows, :] - rate * (wide[rows, :] * scale)).astype(jnp.bfloat16)
+        steps[rows, :] = narrow[rows, :] * scale
+        moves.append(pltpu.make_async_copy(steps.at[rows], step, step_sems.at[k]))
+        moves[-1].start()
+    for move in moves:
+        move.wait()
 
 
 def per_device(
@@ -240,6 +271,7 @@
     tokens = block_in.shape[0]
 
     rows_in_all = 2 * RANK * width // LANES
+    dense = 2 * width * columns // LANES
 
     def exchanged(tiles):
         shape = (PARTS, rows_in_all // PARTS // 2, 2, LANES)
@@ -248,16 +280,17 @@
 
     packed, weights = call(
         pack_kernel,
-        [((columns, 2 * RANK), bf16), ((2 * width, columns), f32, pltpu.HBM)],
+        [((columns, 2 * RANK), bf16), ((dense, LANES), f32, pltpu.HBM)],
         [HBM] * 4,
         4,
         [
             pltpu.VMEM((2, columns, RANK), bf16),
             pltpu.VMEM((2 * width, columns), f32),
+            pltpu.VMEM((dense, LANES), f32),
             pltpu.SemaphoreType.DMA((4,)),
         ],
     )(in_hbm(factor_out), in_hbm(factor_z), in_hbm(weight_out), in_hbm(weight_z.T))
-    weights = lax.all_gather(weights, FS, axis=0, tiled=True).reshape(PARTS, 2 * width, columns)
+    weights = lax.all_gather(weights, FS, axis=0, tiled=True).reshape(PARTS, dense, LANES)
     own = lax.all_gather(packed, "z", axis=0, tiled=True)
     other = lax.ppermute(own, "core", [(0, 1), (1, 0)])
     _, source = lax.optimization_barrier((own, out_cot))
@@ -299,7 +332,7 @@
         [HBM],
         16,
         [
-            pltpu.VMEM((PARTS, 2 * width, columns), f32),
+            pltpu.VMEM((PARTS, dense, LANES), f32),
             pltpu.VMEM((2 * width, D), f32),
             pltpu.SemaphoreType.DMA((2,)),
         ],
@@ -319,9 +352,15 @@
     sums = lax.all_to_all(sums, TP, split_axis=0, concat_axis=0, tiled=True)
     copy_out, copy_z, step_out, step_z = call(
         final_kernel,
-        [((width, D), bf16), ((width, D), bf16), ((width, columns), f32), ((width, columns), f32)],
+        [((width, D), bf16, pltpu.HBM)] * 2 + [((width, columns), f32, pltpu.HBM)] * 2,
         [VMEM] * 4,
         4,
+        [
+            pltpu.VMEM((2 * width, D), bf16),
+            pltpu.VMEM((2 * width, columns), f32),
+            pltpu.SemaphoreType.DMA((2, BANDS)),
+            pltpu.SemaphoreType.DMA((2,)),
+        ],
     )(sums, in_vmem(wide), in_vmem(narrow), in_vmem(full))
     return (
         step_out, step_z.T, news[0].T, news[1].T, news[2], news[3], copy_out, copy_z.T,

time: 129 us -> 128 us (level)
  no operation moved by 1% of the time
where the time goes in v3:
time: 128 us; the launch traced here: 127 us
  blocking collectives  69.8 us (55%)
  Pallas kernels  18.2 us (14%)
  starting transfers between devices  14.6 us (11%)
  between operations  14.2 us (11%)
  waiting for transfers between devices  10.3 us (8%)
    all_gather x1, blocking collectives, per_device(): own = lax.all_gather(packed, 'z', axis=0, tiled=True)  34 us
    all_to_all x1, blocking collectives, per_device(): sums = lax.all_to_all(sums, TP, split_axis=0, concat_axis=0, tiled=True)  18.4 us
    all_to_all x1, blocking collectives, exchanged(): lax.all_to_all(tiles.reshape(shape), FS, split_axis=0, concat_axis=0, til...  17.5 us
    all_to_all x1, waiting for transfers between devices, exchanged(): lax.all_to_all(tiles.reshape(shape), FS, split_axis=0, concat_axis=0, til...  10.3 us
    ppermute x1, starting transfers between devices, per_device(): other = lax.ppermute(own, 'core', [(0, 1), (1, 0)])  8.51 us
    all_to_all x1, starting transfers between devices, exchanged(): lax.all_to_all(tiles.reshape(shape), FS, split_axis=0, concat_axis=0, til...  6.05 us
    pallas_call x1, Pallas kernels, per_device(): call(gradient_kernel, [((rows_in_all, LANES), f32)] + [((D, RANK), bf16,...  5.96 us
    pallas_call x1, Pallas kernels, per_device(): call(ordered_kernel, [((2 * width, D), f32, pltpu.HBM)], [HBM], 16, [pltp...  4.03 us
  transfers between devices with their start and end apart: 3, of which 1 were waited for; matrix products, arithmetic and copies ran while one was open for 0% of the time, Pallas kernels for 10%

profile of v3, /device:TPU:1, one launch (start us, length us, event | category | flops | bytes accessed | tf_op | source)
XLA Modules:
  0.0 127.2 jit_solution(2836620348357651733)
XLA Ops:
  7.2 0.0 all-gather.2.cloned.1.call-start
  7.2 1.7 %shard_map.179 = (bf16[96,384]{1,0:T(8,128)(2,1)S(1)}, f32[216,128]{1,0:T(8,128)}) custom-call(bf16[96,192]{1,0:T(8,128)(2,1)} %factor_out.1, bf16[96,192]{1,0:T(8,128)(2,1)} %factor_z.1, f32[144,96]{1,0:T(8,128)} %weight_out.1, f32[144,96]{1,0:T(8,128)} %bitcast.22), custom_call_target="tpu_custom_call" | custom-call | tf_op jit(solution)/shard_map/pallas_call | solution.py:281
  8.9 0.0 all-gather.2.cloned.1.call-update
  8.9 34.0 %all_gather.6.own = bf16[1152,384]{1,0:T(8,128)(2,1)S(1)} all-gather(bf16[96,384]{1,0:T(8,128)(2,1)S(1)} %get-tuple-element.27), channel_id=1, replica_groups=mesh['z'=12,'core'=2,'y'=8,'x'=4] {'z'}, dimensions={0}, use_global_device_ids=true | all-gather | bytes 958464 | tf_op jit(solution)/shard_map/all_gather | solution.py:294
  42.9 8.5 %collective-permute-start = (bf16[1152,384]{1,0:T(8,128)(2,1)S(1)}, bf16[1152,384]{1,0:T(8,128)(2,1)S(1)}, u32[]{:S(2)}, u32[]{:S(2)}) collective-permute-start(bf16[1152,384]{1,0:T(8,128)(2,1)S(1)} %all_gather.6.own), channel_id=1, source_target_pairs={{0,32},{32,0},{1,33},{33,1},{2,34},{34,2},{3,35},{35,3},{4,36},{36... | collective-permute-start | bytes 2654216 | tf_op jit(solution)/shard_map/ppermute | solution.py:295
  51.4 2.4 %shard_map.180.cot = bf16[1024,2304]{1,0:T(8,128)(2,1)S(1)} custom-call(bf16[1024,2304]{1,0:T(8,128)(2,1)} %source), custom_call_target="tpu_custom_call" | custom-call | tf_op jit(solution)/shard_map/pallas_call | solution.py:297
  53.8 0.0 collective-permute-done.other
  53.8 0.0 copy-start
  53.9 0.0 copy-start.1
  53.9 0.0 copy-start.2
  53.9 0.0 copy-start.3
  53.9 6.0 %shard_map.181 = (f32[432,128]{1,0:T(8,128)S(1)}, bf16[2304,192]{1,0:T(8,128)(2,1)S(1)}, bf16[2304,192]{1,0:T(8,128)(2,1)S(1)}) custom-call(bf16[1024,2304]{1,0:T(8,128)(2,1)S(1)} %shard_map.180.cot, bf16[1024,2304]{1,0:T(8,128)(2,1)} %inp.1, bf16[1152,384]{1,0:T(8,128)(2,1)S(1)} %all_gather.6.own, bf16[1152,384]{1,0:T(8,128)(2,1)S(1)} %collective-permute-done.other, ...), custom_call_target="tpu_custom_call" | custom-call | tf_op jit(solution)/shard_map/pallas_call | solution.py:305
  59.9 17.5 %all_to_all.15 = f32[24,9,2,128]{3,2,1,0:T(2,128)S(1)} all-to-all(f32[24,9,2,128]{3,2,1,0:T(2,128)S(1)} %bitcast.16), channel_id=1, replica_groups=mesh['z'=12,'core'=2,'y'=8,'x'=4] {'z','core'}, dimensions={0} | all-to-all | bytes 442368 | tf_op jit(solution)/shard_map/all_to_all | solution.py:278
  77.3 0.0 copy-done
  77.3 0.0 copy-done.1
  77.3 0.0 copy-done.2
  77.3 0.0 copy-done.3
  77.4 0.9 shard_map.182
  78.3 6.1 %all-to-all-start.1 = ((f32[24,9,2,128]{3,2,1,0:T(2,128)}), f32[24,9,2,128]{3,2,1,0:T(2,128)S(1)}, u32[]{:S(2)}, u32[]{:S(2)}) async-start(f32[24,9,2,128]{3,2,1,0:T(2,128)} %bitcast.7), calls=%async_computation.1 | async-start | bytes 442368 | tf_op jit(solution)/shard_map/all_to_all | solution.py:278
  84.3 0.0 all-gather.2.cloned.1.call-done
  84.4 4.0 %shard_map.183.ordered = f32[288,2304]{1,0:T(8,128)} custom-call(f32[24,216,128]{2,1,0:T(8,128)} %bitcast.19), custom_call_target="tpu_custom_call" | custom-call | tf_op jit(solution)/shard_map/pallas_call | solution.py:329
  88.4 10.3 %all-to-all-done.1 = f32[24,9,2,128]{3,2,1,0:T(2,128)S(1)} async-done(((f32[24,9,2,128]{3,2,1,0:T(2,128)}), f32[24,9,2,128]{3,2,1,0:T(2,128)S(1)}, u32[]{:S(2)}, u32[]{:S(2)}) %all-to-all-start.1) | async-done | bytes 221216 | tf_op jit(solution)/shard_map/all_to_all | solution.py:278
  98.7 1.8 %shard_map.184 = (f32[288,2304]{1,0:T(8,128)S(1)}, f32[288,96]{1,0:T(8,128)S(1)}, f32[288,2304]{1,0:T(8,128)S(1)}, f32[32,1,128]{2,1,0:T(1,128)S(1)}) custom-call(f32[432,128]{1,0:T(8,128)S(1)} %bitcast.15, bf16[2304,192]{1,0:T(8,128)(2,1)S(1)} %get-tuple-element.31.factor_out, bf16[2304,192]{1,0:T(8,128)(2,1)S(1)} %get-tuple-element.32.factor_z, ...), custom_call_target="tpu_custom_call" | custom-call | tf_op jit(solution)/shard_map/pallas_call | solution.py:340
  100.5 18.4 %all_to_all.16.sums = f32[32,1,128]{2,1,0:T(1,128)S(1)} all-to-all(f32[32,1,128]{2,1,0:T(1,128)S(1)} %get-tuple-element.34), channel_id=1, replica_groups=mesh['z'=12,'core'=2,'y'=8,'x'=4] {'y','x'}, dimensions={0} | all-to-all | bytes 32768 | tf_op jit(solution)/shard_map/all_to_all | solution.py:352
  118.8 1.4 %shard_map.185 = (bf16[144,2304]{1,0:T(8,128)(2,1)}, bf16[144,2304]{1,0:T(8,128)(2,1)}, f32[144,96]{1,0:T(8,128)}, f32[144,96]{1,0:T(8,128)}) custom-call(f32[32,1,128]{2,1,0:T(1,128)S(1)} %all_to_all.16.sums, f32[288,2304]{1,0:T(8,128)S(1)} %get-tuple-element.35.wide, f32[288,96]{1,0:T(8,128)S(1)} %get-tuple-element.36.narrow, ...), custom_call_target="tpu_custom_call" | custom-call | tf_op jit(solution)/shard_map/pallas_call | solution.py:353
Async XLA Ops:
  7.2 77.2 %all-gather.2.cloned.1.call-start = ((), (), s32[]{:S(2)}) async-start(), calls=%async_computation.3 | async-start | bytes 2764800 | tf_op jit(solution)/shard_map/all_gather | solution.py:293
  42.9 10.9 %collective-permute-start = (bf16[1152,384]{1,0:T(8,128)(2,1)S(1)}, bf16[1152,384]{1,0:T(8,128)(2,1)S(1)}, u32[]{:S(2)}, u32[]{:S(2)}) collective-permute-start(bf16[1152,384]{1,0:T(8,128)(2,1)S(1)} %all_gather.6.own), channel_id=1, source_target_pairs={{0,32},{32,0},{1,33},{33,1},{2,34},{34,2},{3,35},{35,3},{4,36},{36... | collective-permute-start | bytes 2654216 | tf_op jit(solution)/shard_map/ppermute | solution.py:295
  53.8 23.5 %copy-start = (f32[144,8]{0,1:T(8,128)S(1)}, f32[144,8]{0,1:T(8,128)}, u32[]{:S(2)}) copy-start(f32[144,8]{0,1:T(8,128)} %param.20) | copy-start | bytes 13828
  53.9 23.5 %copy-start.1 = (f32[144,8]{0,1:T(8,128)S(1)}, f32[144,8]{0,1:T(8,128)}, u32[]{:S(2)}) copy-start(f32[144,8]{0,1:T(8,128)} %param.21) | copy-start | bytes 13828
  53.9 23.5 %copy-start.2 = (f32[8,144]{1,0:T(8,128)S(1)}, f32[8,144]{1,0:T(8,128)}, u32[]{:S(2)}) copy-start(f32[8,144]{1,0:T(8,128)} %first_z.1) | copy-start | bytes 13828
  53.9 23.5 %copy-start.3 = (f32[8,144]{1,0:T(8,128)S(1)}, f32[8,144]{1,0:T(8,128)}, u32[]{:S(2)}) copy-start(f32[8,144]{1,0:T(8,128)} %second_z.1) | copy-start | bytes 13828
  78.3 20.4 %all-to-all-start.1 = ((f32[24,9,2,128]{3,2,1,0:T(2,128)}), f32[24,9,2,128]{3,2,1,0:T(2,128)S(1)}, u32[]{:S(2)}, u32[]{:S(2)}) async-start(f32[24,9,2,128]{3,2,1,0:T(2,128)} %bitcast.7), calls=%async_computation.1 | async-start | bytes 442368 | tf_op jit(solution)/shard_map/all_to_all | solution.py:278
Sparse Core Ops, SparseCore 0:
  11.0 70.5 all-gather.1

commit v4 on v3

--- a/solution.py
+++ b/solution.py
@@ -5,6 +5,7 @@
 from jax.experimental.pallas import tpu as pltpu
 from jax.sharding import Mesh
 from jax.sharding import PartitionSpec as P
+
 
 D = 2304
 INNER = 4608
@@ -185,26 +186,28 @@
         tiles[each * p : each * (p + 1), :] = part[...]
 
 
-def ordered_kernel(weights, ordered, blocks, full, sems):
-    rows, columns = blocks.shape[1], full.shape[1] // PARTS
+def gate_kernel(value, source, kept):
+    del value, source, kept
+
+
+def ordered_kernel(own, other, ordered, blocks, full, sems):
+    rows, columns = blocks.shape[2], full.shape[1] // PARTS
     quarter, spare = full.shape[0] - rows, LANES - columns
-    half = PARTS // 2
+    here = lax.axis_index("core")
     moves = [
-        pltpu.make_async_copy(
-            weights.at[pl.ds(half * k, half)], blocks.at[pl.ds(half * k, half)], sems.at[k]
-        )
-        for k in range(2)
+        pltpu.make_async_copy(own, blocks.at[:, here], sems.at[0]),
+        pltpu.make_async_copy(other, blocks.at[:, 1 - here], sems.at[1]),
     ]
     for move in moves:
         move.start()
+    for move in moves:
+        move.wait()
     for k in range(PARTS):
-        if k % half == 0:
-            moves[k // half].wait()
-        at = k * columns
-        full[:rows, at : at + columns] = blocks[k, :, :columns]
+        at, block = k * columns, blocks.at[k // CORES, k % CORES]
+        full[:rows, at : at + columns] = block[:, :columns]
         for j in range(rows // quarter):
-            full[rows:, at + spare * j : at + spare * (j + 1)] = blocks[
-                k, quarter * j : quarter * (j + 1), columns:
+            full[rows:, at + spare * j : at + spare * (j + 1)] = block[
+                quarter * j : quarter * (j + 1), columns:
             ]
     out = pltpu.make_async_copy(full, ordered, sems.at[0])
     out.start()
@@ -290,7 +293,7 @@
             pltpu.SemaphoreType.DMA((4,)),
         ],
     )(in_hbm(factor_out), in_hbm(factor_z), in_hbm(weight_out), in_hbm(weight_z.T))
-    weights = lax.all_gather(weights, FS, axis=0, tiled=True).reshape(PARTS, dense, LANES)
+    weights = lax.all_gather(weights, "z", axis=0, tiled=True)
     own = lax.all_gather(packed, "z", axis=0, tiled=True)
     other = lax.ppermute(own, "core", [(0, 1), (1, 0)])
     _, source = lax.optimization_barrier((own, out_cot))
@@ -325,18 +328,27 @@
         4,
         [pltpu.VMEM((rows_in_all // PARTS, LANES), f32), pltpu.VMEM((ranks, width), f32)],
     )(arrived, first_out.T, second_out.T, first_z, second_z)
+    weights = pl.pallas_call(
+        gate_kernel,
+        out_shape=pltpu.HBM(weights.shape, f32),
+        in_specs=[HBM, HBM],
+        out_specs=HBM,
+        input_output_aliases={1: 0},
+    )(in_hbm(news[2]), in_hbm(weights))
     ratios = exchanged(ratios)
+    others = lax.ppermute(weights, "core", [(0, 1), (1, 0)])
+    blocks = (RINGS, dense, LANES)
     (ordered,) = call(
         ordered_kernel,
         [((2 * width, D), f32, pltpu.HBM)],
-        [HBM],
+        [HBM] * 2,
         16,
         [
-            pltpu.VMEM((PARTS, dense, LANES), f32),
+            pltpu.VMEM((RINGS, CORES, dense, LANES), f32),
             pltpu.VMEM((2 * width, D), f32),
             pltpu.SemaphoreType.DMA((2,)),
         ],
-    )(in_hbm(weights))
+    )(in_hbm(weights.reshape(blocks)), in_hbm(others.reshape(blocks)))
     wide, narrow, full, sums = call(
         update_kernel,
         [

time: 128 us -> 133 us (1.039)
  starting transfers between devices: 14.6 us -> 20.6 us
    ppermute x0 -> x1, starting transfers between devices: none -> 4.67 us  [per_device(): others = lax.ppermute(weights, 'core', [(0, 1), (1, 0)])]
    all_to_all x1, starting transfers between devices: 6.05 us -> 7.47 us  [exchanged(): lax.all_to_all(tiles.reshape(shape), FS, split_axis=0, concat_axis=0, til...]
    all_to_all x1, blocking collectives: 18.4 us -> 17 us  [per_device(): sums = lax.all_to_all(sums, TP, split_axis=0, concat_axis=0, tiled=True)]
    pallas_call x1 -> x2, Pallas kernels: 4.03 us -> 4.35 us  [the longest x1 4.35 us: per_device(): call(ordered_kernel, [((2 * width, D), f32, pltpu.HBM)], [HBM] * 2, 16, [...]
  transfers between devices with their start and end apart: 3 -> 4, of which waited for: 1 -> 1; matrix products, arithmetic and copies ran while one was open for 0% -> 0% of each run, Pallas kernels for 10% -> 10%
where the time goes in v4:
time: 133 us; the launch traced here: 132 us
  blocking collectives  68.8 us (52%)
  starting transfers between devices  20.6 us (15%)
  Pallas kernels  18.4 us (14%)
  between operations  14.2 us (11%)
  waiting for transfers between devices  10 us (8%)
    all_gather x1, blocking collectives, per_device(): own = lax.all_gather(packed, 'z', axis=0, tiled=True)  34 us
    all_to_all x1, blocking collectives, exchanged(): lax.all_to_all(tiles.reshape(shape), FS, split_axis=0, concat_axis=0, til...  17.8 us
    all_to_all x1, blocking collectives, per_device(): sums = lax.all_to_all(sums, TP, split_axis=0, concat_axis=0, tiled=True)  17 us
    all_to_all x1, waiting for transfers between devices, exchanged(): lax.all_to_all(tiles.reshape(shape), FS, split_axis=0, concat_axis=0, til...  10 us
    ppermute x1, starting transfers between devices, per_device(): other = lax.ppermute(own, 'core', [(0, 1), (1, 0)])  8.48 us
    all_to_all x1, starting transfers between devices, exchanged(): lax.all_to_all(tiles.reshape(shape), FS, split_axis=0, concat_axis=0, til...  7.47 us
    pallas_call x1, Pallas kernels, per_device(): call(gradient_kernel, [((rows_in_all, LANES), f32)] + [((D, RANK), bf16,...  5.92 us
    ppermute x1, starting transfers between devices, per_device(): others = lax.ppermute(weights, 'core', [(0, 1), (1, 0)])  4.67 us
  transfers between devices with their start and end apart: 4, of which 1 were waited for; matrix products, arithmetic and copies ran while one was open for 0% of the time, Pallas kernels for 10%

profile of v4, /device:TPU:1, one launch (start us, length us, event | category | flops | bytes accessed | tf_op | source)
XLA Modules:
  0.0 132.1 jit_solution(10980588653863136654)
XLA Ops:
  7.2 0.0 all-gather.2.cloned.1.call-start
  7.2 1.7 %shard_map.179 = (bf16[96,384]{1,0:T(8,128)(2,1)S(1)}, f32[216,128]{1,0:T(8,128)}) custom-call(bf16[96,192]{1,0:T(8,128)(2,1)} %factor_out.1, bf16[96,192]{1,0:T(8,128)(2,1)} %factor_z.1, f32[144,96]{1,0:T(8,128)} %weight_out.1, f32[144,96]{1,0:T(8,128)} %bitcast.23), custom_call_target="tpu_custom_call" | custom-call | tf_op jit(solution)/shard_map/pallas_call | solution.py:284
  8.9 0.0 all-gather.2.cloned.1.call-update
  8.9 34.0 %all_gather.6.own = bf16[1152,384]{1,0:T(8,128)(2,1)S(1)} all-gather(bf16[96,384]{1,0:T(8,128)(2,1)S(1)} %get-tuple-element.27), channel_id=1, replica_groups=mesh['z'=12,'core'=2,'y'=8,'x'=4] {'z'}, dimensions={0}, use_global_device_ids=true | all-gather | bytes 958464 | tf_op jit(solution)/shard_map/all_gather | solution.py:297
  42.9 8.5 %collective-permute-start = (bf16[1152,384]{1,0:T(8,128)(2,1)S(1)}, bf16[1152,384]{1,0:T(8,128)(2,1)S(1)}, u32[]{:S(2)}, u32[]{:S(2)}) collective-permute-start(bf16[1152,384]{1,0:T(8,128)(2,1)S(1)} %all_gather.6.own), channel_id=1, source_target_pairs={{0,32},{32,0},{1,33},{33,1},{2,34},{34,2},{3,35},{35,3},{4,36},{36... | collective-permute-start | bytes 2654216 | tf_op jit(solution)/shard_map/ppermute | solution.py:298
  51.4 2.4 %shard_map.180.cot = bf16[1024,2304]{1,0:T(8,128)(2,1)S(1)} custom-call(bf16[1024,2304]{1,0:T(8,128)(2,1)} %source), custom_call_target="tpu_custom_call" | custom-call | tf_op jit(solution)/shard_map/pallas_call | solution.py:300
  53.8 0.0 collective-permute-done.other
  53.8 0.0 copy-start
  53.8 0.0 copy-start.1
  53.8 0.0 copy-start.2
  53.8 0.0 copy-start.3
  53.8 5.9 %shard_map.181 = (f32[432,128]{1,0:T(8,128)S(1)}, bf16[2304,192]{1,0:T(8,128)(2,1)S(1)}, bf16[2304,192]{1,0:T(8,128)(2,1)S(1)}) custom-call(bf16[1024,2304]{1,0:T(8,128)(2,1)S(1)} %shard_map.180.cot, bf16[1024,2304]{1,0:T(8,128)(2,1)} %inp.1, bf16[1152,384]{1,0:T(8,128)(2,1)S(1)} %all_gather.6.own, bf16[1152,384]{1,0:T(8,128)(2,1)S(1)} %collective-permute-done.other, ...), custom_call_target="tpu_custom_call" | custom-call | tf_op jit(solution)/shard_map/pallas_call | solution.py:308
  59.8 17.8 %all_to_all.15 = f32[24,9,2,128]{3,2,1,0:T(2,128)S(1)} all-to-all(f32[24,9,2,128]{3,2,1,0:T(2,128)S(1)} %bitcast.17), channel_id=1, replica_groups=mesh['z'=12,'core'=2,'y'=8,'x'=4] {'z','core'}, dimensions={0} | all-to-all | bytes 442368 | tf_op jit(solution)/shard_map/all_to_all | solution.py:281
  77.6 0.0 copy-done
  77.6 0.0 copy-done.1
  77.6 0.0 copy-done.2
  77.6 0.0 copy-done.3
  77.6 0.9 shard_map.182
  78.5 0.0 all-gather.2.cloned.1.call-done.source
  78.5 4.7 %collective-permute-start.1 = (f32[2592,128]{1,0:T(8,128)}, f32[2592,128]{1,0:T(8,128)}, u32[]{:S(2)}, u32[]{:S(2)}) collective-permute-start(f32[2592,128]{1,0:T(8,128)} %shard_map.183), channel_id=1, source_target_pairs={{0,32},{32,0},{1,33},{33,1},{2,34},{34,2},{3,35},{35,3},{4,36},{36... | collective-permute-start | bytes 3981320 | tf_op jit(solution)/shard_map/ppermute | solution.py:339
  83.2 7.5 %all-to-all-start.1 = ((f32[24,9,2,128]{3,2,1,0:T(2,128)}), f32[24,9,2,128]{3,2,1,0:T(2,128)S(1)}, u32[]{:S(2)}, u32[]{:S(2)}) async-start(f32[24,9,2,128]{3,2,1,0:T(2,128)} %bitcast.7), calls=%async_computation.1 | async-start | bytes 442368 | tf_op jit(solution)/shard_map/all_to_all | solution.py:281
  90.7 0.0 collective-permute-done.1
  90.7 4.3 %shard_map.184.ordered = f32[288,2304]{1,0:T(8,128)} custom-call(f32[12,216,128]{2,1,0:T(8,128)} %bitcast.20, f32[12,216,128]{2,1,0:T(8,128)} %bitcast.10.other), custom_call_target="tpu_custom_call" | custom-call | tf_op jit(solution)/shard_map/pallas_call | solution.py:341
  95.0 10.0 %all-to-all-done.1 = f32[24,9,2,128]{3,2,1,0:T(2,128)S(1)} async-done(((f32[24,9,2,128]{3,2,1,0:T(2,128)}), f32[24,9,2,128]{3,2,1,0:T(2,128)S(1)}, u32[]{:S(2)}, u32[]{:S(2)}) %all-to-all-start.1) | async-done | bytes 221216 | tf_op jit(solution)/shard_map/all_to_all | solution.py:281
  105.0 1.8 %shard_map.185 = (f32[288,2304]{1,0:T(8,128)S(1)}, f32[288,96]{1,0:T(8,128)S(1)}, f32[288,2304]{1,0:T(8,128)S(1)}, f32[32,1,128]{2,1,0:T(1,128)S(1)}) custom-call(f32[432,128]{1,0:T(8,128)S(1)} %bitcast.16, bf16[2304,192]{1,0:T(8,128)(2,1)S(1)} %get-tuple-element.31.factor_out, bf16[2304,192]{1,0:T(8,128)(2,1)S(1)} %get-tuple-element.32.factor_z, ...), custom_call_target="tpu_custom_call" | custom-call | tf_op jit(solution)/shard_map/pallas_call | solution.py:352
  106.8 17.0 %all_to_all.16.sums = f32[32,1,128]{2,1,0:T(1,128)S(1)} all-to-all(f32[32,1,128]{2,1,0:T(1,128)S(1)} %get-tuple-element.35), channel_id=1, replica_groups=mesh['z'=12,'core'=2,'y'=8,'x'=4] {'y','x'}, dimensions={0} | all-to-all | bytes 32768 | tf_op jit(solution)/shard_map/all_to_all | solution.py:364
  123.9 1.4 %shard_map.186 = (bf16[144,2304]{1,0:T(8,128)(2,1)}, bf16[144,2304]{1,0:T(8,128)(2,1)}, f32[144,96]{1,0:T(8,128)}, f32[144,96]{1,0:T(8,128)}) custom-call(f32[32,1,128]{2,1,0:T(1,128)S(1)} %all_to_all.16.sums, f32[288,2304]{1,0:T(8,128)S(1)} %get-tuple-element.36.wide, f32[288,96]{1,0:T(8,128)S(1)} %get-tuple-element.37.narrow, ...), custom_call_target="tpu_custom_call" | custom-call | tf_op jit(solution)/shard_map/pallas_call | solution.py:365
  (1 shorter events, 0.0 us)
Async XLA Ops:
  7.2 71.4 %all-gather.2.cloned.1.call-start = ((), (), s32[]{:S(2)}) async-start(), calls=%async_computation.3 | async-start | bytes 1437696 | tf_op jit(solution)/shard_map/all_gather | solution.py:296
  42.9 10.9 %collective-permute-start = (bf16[1152,384]{1,0:T(8,128)(2,1)S(1)}, bf16[1152,384]{1,0:T(8,128)(2,1)S(1)}, u32[]{:S(2)}, u32[]{:S(2)}) collective-permute-start(bf16[1152,384]{1,0:T(8,128)(2,1)S(1)} %all_gather.6.own), channel_id=1, source_target_pairs={{0,32},{32,0},{1,33},{33,1},{2,34},{34,2},{3,35},{35,3},{4,36},{36... | collective-permute-start | bytes 2654216 | tf_op jit(solution)/shard_map/ppermute | solution.py:298
  53.8 23.8 %copy-start = (f32[144,8]{0,1:T(8,128)S(1)}, f32[144,8]{0,1:T(8,128)}, u32[]{:S(2)}) copy-start(f32[144,8]{0,1:T(8,128)} %param.20) | copy-start | bytes 13828
  53.8 23.8 %copy-start.1 = (f32[144,8]{0,1:T(8,128)S(1)}, f32[144,8]{0,1:T(8,128)}, u32[]{:S(2)}) copy-start(f32[144,8]{0,1:T(8,128)} %param.21) | copy-start | bytes 13828
  53.8 23.8 %copy-start.2 = (f32[8,144]{1,0:T(8,128)S(1)}, f32[8,144]{1,0:T(8,128)}, u32[]{:S(2)}) copy-start(f32[8,144]{1,0:T(8,128)} %first_z.1) | copy-start | bytes 13828
  53.8 23.8 %copy-start.3 = (f32[8,144]{1,0:T(8,128)S(1)}, f32[8,144]{1,0:T(8,128)}, u32[]{:S(2)}) copy-start(f32[8,144]{1,0:T(8,128)} %second_z.1) | copy-start | bytes 13828
  78.5 12.2 %collective-permute-start.1 = (f32[2592,128]{1,0:T(8,128)}, f32[2592,128]{1,0:T(8,128)}, u32[]{:S(2)}, u32[]{:S(2)}) collective-permute-start(f32[2592,128]{1,0:T(8,128)} %shard_map.183), channel_id=1, source_target_pairs={{0,32},{32,0},{1,33},{33,1},{2,34},{34,2},{3,35},{35,3},{4,36},{36... | collective-permute-start | bytes 3981320 | tf_op jit(solution)/shard_map/ppermute | solution.py:339
  83.2 21.8 %all-to-all-start.1 = ((f32[24,9,2,128]{3,2,1,0:T(2,128)}), f32[24,9,2,128]{3,2,1,0:T(2,128)S(1)}, u32[]{:S(2)}, u32[]{:S(2)}) async-start(f32[24,9,2,128]{3,2,1,0:T(2,128)} %bitcast.7), calls=%async_computation.1 | async-start | bytes 442368 | tf_op jit(solution)/shard_map/all_to_all | solution.py:281
Sparse Core Ops, SparseCore 0:
  10.9 63.0 all-gather.1
